TPU v7x, 32 devices: a whole 2x2x4 slice. The times are simulated.
32 devices in a mesh: ep: 8 (over z, core), tp: 4 (over y, x).
Axes of the slice: x: 2, y: 2, z: 4, core: 2. Of those that a mesh axis runs over, the one named last changes fastest.
Arguments:
- mix_input: bfloat16 [1024, 2048], P('ep'), may hold values from -8 to 8
- expert_input: bfloat16 [1024, 2048], P('ep'), may hold values from -8 to 8
- mix_gain: float32 [2048], replicated, may hold values from 0.1 to 1.9
- moe_gain: float32 [2048], replicated, may hold values from 0.1 to 1.9
- pool_in: bfloat16 [2048, 1024], P(None, 'tp'), may hold values from -0.125 to 0.125
- pool_scale: float32 [1024], P('tp'), may hold values from 0.25 to 10
- pool_gain: float32 [1024], P('tp'), may hold values from 0.1 to 1.9
- pool_out: bfloat16 [1024, 2048], P(None, 'tp'), may hold values from -0.1875 to 0.1875
- route: int32 [1024, 4], P('ep'), may hold values from 0 to 7, all different within a row; in each aligned block of 128 rows (0 to 127, 128 to 255, ...) at most 128 rows name the same one
- route_score: float32 [1024, 4], P('ep'), may hold values from 0.05 to 1
- expert_gate: bfloat16 [8, 2048, 2048], P('ep', None, 'tp'), may hold values from -0.125 to 0.125
- expert_up: bfloat16 [8, 2048, 2048], P('ep', None, 'tp'), may hold values from -0.125 to 0.125
- expert_down: bfloat16 [8, 2048, 2048], P('ep', 'tp'), may hold values from -0.1875 to 0.1875
- shared_gate: bfloat16 [2048, 2048], P(None, 'tp'), may hold values from -0.125 to 0.125
- shared_up: bfloat16 [2048, 2048], P(None, 'tp'), may hold values from -0.125 to 0.125
- shared_down: bfloat16 [2048, 2048], P(None, 'tp'), may hold values from -0.125 to 0.125
Outputs:
- mix_out: bfloat16 [1024, 2048], P('ep', 'tp')
- moe_out: bfloat16 [1024, 2048], P('ep', 'tp')
Inputs may be any that keep to these rules, and one draw needn't show every extreme that they name: `route`: each row names 4 different experts. In the rows of one index of ep (aligned blocks of 128 rows) no expert is named more than 128 times, a bound that some block reaches.
All inputs are finite; a program needn't handle non-finite values.
Results may differ from a plain program's by a relative error of at most 0.014.
Values may be sent and summed in bfloat16 or wider, within the bound.
A program may use at most 64 MiB of HBM per device.

v0:
```python
import jax
import jax.numpy as jnp
from jax import lax
from jax.sharding import PartitionSpec as P

epsilon = 1e-06
reach_rows = 15
window_widths = (2, 4, 8, 16)


def shifted(block, axis, distance):
    devices = range(lax.axis_size(axis))
    route = [(i - distance, i) for i in devices if i - distance in devices]
    return lax.ppermute(block, axis, route)


def row_norm(rows, gain):
    values = rows.astype(jnp.float32)
    scale = lax.rsqrt(jnp.mean(values * values, axis=-1, keepdims=True) + epsilon)
    return (values * scale * gain).astype(jnp.bfloat16)


def window_means(extended, position, group, n_rows):
    total = jnp.zeros((n_rows, extended.shape[1]), jnp.float32)
    result = jnp.zeros((n_rows, extended.shape[1]), jnp.float32)
    for lag in range(16):
        total = total + extended[reach_rows - lag : reach_rows - lag + n_rows]
        for index, width in enumerate(window_widths):
            if lag + 1 == width:
                count = jnp.minimum(position, float(width))[:, None]
                result = jnp.where(group[None, :] == index, total / count, result)
    return result - extended[reach_rows:]


def serve(sending, expert_gate, expert_up, expert_down):
    arrived = lax.all_to_all(sending, "ep", split_axis=0, concat_axis=0, tiled=True)
    gate = jnp.einsum("send,edf->senf", arrived, expert_gate, preferred_element_type=jnp.float32)
    upper = jnp.einsum("send,edf->senf", arrived, expert_up, preferred_element_type=jnp.float32)
    hidden = (jax.nn.silu(gate) * upper).astype(jnp.bfloat16)
    term = jnp.einsum("senf,efd->send", hidden, expert_down, preferred_element_type=jnp.float32)
    summed = lax.psum_scatter(term.astype(jnp.bfloat16), "tp", scatter_dimension=3, tiled=True)
    return lax.all_to_all(summed, "ep", split_axis=0, concat_axis=0, tiled=True)


def on_device(
    mix_input,
    expert_input,
    mix_gain,
    moe_gain,
    pool_in,
    pool_scale,
    pool_gain,
    pool_out,
    route,
    route_score,
    expert_gate,
    expert_up,
    expert_down,
    shared_gate,
    shared_up,
    shared_down,
):
    tok_rows = mix_input.shape[0]
    channels = pool_in.shape[1]
    pool_width = channels * lax.axis_size("tp")
    mix_norm = row_norm(mix_input, mix_gain)
    pool_input = jnp.dot(mix_norm, pool_in, preferred_element_type=jnp.float32).astype(jnp.bfloat16)
    before = shifted(pool_input[tok_rows - reach_rows :], "ep", 1)
    extended = jnp.concatenate([before, pool_input], axis=0).astype(jnp.float32)
    position = (lax.axis_index("ep") * tok_rows + jnp.arange(tok_rows, dtype=jnp.int32) + 1).astype(
        jnp.float32
    )
    channel_ids = lax.axis_index("tp") * channels + jnp.arange(channels, dtype=jnp.int32)
    group = channel_ids // (pool_width // 4)
    scaled = window_means(extended, position, group, tok_rows) * pool_scale
    squares = lax.psum(jnp.sum(scaled * scaled, axis=1), "tp")
    pooled_norm = (scaled * lax.rsqrt(squares / pool_width + epsilon)[:, None] * pool_gain).astype(
        jnp.bfloat16
    )
    moe_norm = row_norm(expert_input, moe_gain)
    shared_hidden = (
        jax.nn.silu(jnp.dot(moe_norm, shared_gate, preferred_element_type=jnp.float32))
        * jnp.dot(moe_norm, shared_up, preferred_element_type=jnp.float32)
    ).astype(jnp.bfloat16)
    pooled_all, shared_all = (
        lax.all_gather(pooled_norm, "tp", axis=1, tiled=True),
        lax.all_gather(shared_hidden, "tp", axis=1, tiled=True),
    )
    mix_out = jnp.dot(pooled_all, pool_out, preferred_element_type=jnp.float32).astype(jnp.bfloat16)
    shared_part = jnp.dot(shared_all, shared_down, preferred_element_type=jnp.float32)
    n_tok, top = route.shape
    local_experts = expert_gate.shape[0]
    experts = local_experts * lax.axis_size("ep")
    capacity = 2 * n_tok * top // experts
    flat_route = route.reshape(-1)
    table = (flat_route[:, None] == jnp.arange(experts, dtype=jnp.int32)[None, :]).astype(jnp.int32)
    ranks = jnp.sum((jnp.cumsum(table, axis=0) - table) * table, axis=1)
    slot = flat_route * capacity + ranks
    owner = (
        jnp.full((experts * capacity,), n_tok, jnp.int32)
        .at[slot]
        .set(jnp.arange(n_tok * top, dtype=jnp.int32) // top)
    )
    padded_rows = jnp.concatenate(
        [moe_norm, jnp.zeros((1, moe_norm.shape[1]), jnp.bfloat16)], axis=0
    )
    outgoing = padded_rows[owner].reshape(
        lax.axis_size("ep"), local_experts, capacity, moe_norm.shape[1]
    )
    middle = capacity // 2
    first = serve(outgoing[:, :, :middle], expert_gate, expert_up, expert_down)
    second = serve(outgoing[:, :, middle:], expert_gate, expert_up, expert_down)
    returned = jnp.concatenate([first, second], axis=2)
    back_rows = returned.reshape(experts * capacity, returned.shape[3])
    picked = back_rows[slot].reshape(n_tok, top, returned.shape[3]).astype(jnp.float32)
    weights = 2.5 * route_score / jnp.sum(route_score, axis=1, keepdims=True)
    routed = jnp.sum(picked * weights[:, :, None], axis=1)
    moe_out = (routed + shared_part).astype(jnp.bfloat16)
    return (mix_out, moe_out)


def solution(mesh):
    return jax.shard_map(
        on_device,
        mesh=mesh,
        in_specs=(
            P("ep", None),
            P("ep", None),
            P(),
            P(),
            P(None, "tp"),
            P("tp"),
            P("tp"),
            P(None, "tp"),
            P("ep", None),
            P("ep", None),
            P("ep", None, "tp"),
            P("ep", None, "tp"),
            P("ep", "tp", None),
            P(None, "tp"),
            P(None, "tp"),
            P(None, "tp"),
        ),
        out_specs=(P("ep", "tp"), P("ep", "tp")),
        check_vma=False,
    )
```

profile of v0, /device:TPU:0, one launch (start us, length us, event | category | flops | bytes accessed | tf_op | source)
XLA Modules:
  0.0 223.1 jit_solution(1596162430017472814)
XLA Ops:
  10.8 2.4 %scatter_custom_fusion = s32[1024]{0:T(1024)S(1)} fusion(s32[512]{0:T(512)S(1)} %bitcast.166, s32[512]{0:T(512)S(1)} %add_select_fusion, s32[]{:T(128)} %constant.80.clone.1), kind=kCustom, calls=%fused_computation.93 | custom fusion | bytes 4100 | tf_op jit(solution)/shard_map/scatter | solution.py:102
  15.8 6.0 %gather_fusion = bf16[1024,2048]{1,0:T(8,128)(2,1)} fusion(bf16[129,2048]{1,0:T(8,128)(2,1)S(1)} %concatenate.10, s32[1024]{0:T(1024)S(1)} %fusion.94), kind=kCustom, calls=%fused_computation | custom fusion | bytes 8392704 | tf_op jit(solution)/shard_map/gather | solution.py:107
  21.8 4.1 %fusion.103 = (bf16[8,1,64,2048]{3,2,1,0:T(8,128)(2,1)S(1)}, bf16[8,1,64,2048]{3,2,1,0:T(8,128)(2,1)}) fusion(bf16[8,1,128,2048]{3,2,1,0:T(8,128)(2,1)} %bitcast.163), kind=kLoop, calls=%fused_computation.115 | loop fusion | bytes 8388608 | tf_op jit(solution)/shard_map/slice | solution.py:111
  25.9 55.3 %all_to_all.20 = bf16[8,1,64,2048]{3,2,1,0:T(8,128)(2,1)} all-to-all(bf16[8,1,64,2048]{3,2,1,0:T(8,128)(2,1)S(1)} %get-tuple-element.4), channel_id=1, replica_groups=mesh['ep'=8,'tp'=4] {'ep'}, dimensions={0} | all-to-all | bytes 4194304 | tf_op jit(solution)/shard_map/all_to_all | solution.py:36
  81.2 4.4 %all-to-all-start.2 = ((bf16[8,1,64,2048]{3,2,1,0:T(8,128)(2,1)}), bf16[8,1,64,2048]{3,2,1,0:T(8,128)(2,1)}, u32[]{:S(2)}, u32[]{:S(2)}) async-start(bf16[8,1,64,2048]{3,2,1,0:T(8,128)(2,1)} %get-tuple-element.5), calls=%async_computation.3 | async-start | bytes 4194304 | tf_op jit(solution)/shard_map/all_to_all | solution.py:36
  85.6 4.5 %fusion.16 = f32[8,1,64,512]{3,2,0,1:T(8,128)} fusion(bf16[1,2048,512]{2,1,0:T(8,128)(2,1)} %param.26, bf16[8,1,64,2048]{3,2,1,0:T(8,128)(2,1)} %all_to_all.20), kind=kOutput, calls=%fused_computation.21 | convolution fusion | flops 1073741824 | bytes 5242880 | tf_op jit(solution)/shard_map/send,edf->senf/dot_general | solution.py:37
  90.1 6.3 %fusion = bf16[8,1,64,2048]{3,2,0,1:T(8,128)(2,1)} fusion(bf16[1,512,2048]{2,1,0:T(8,128)(2,1)S(1)} %copy-done, bf16[1,2048,512]{2,1,0:T(8,128)(2,1)} %param.27, bf16[8,1,64,2048]{3,2,1,0:T(8,128)(2,1)} %all_to_all.20, f32[8,1,64,512]{3,2,0,1:T(8,128)} %fusion.16), kind=kOutput, calls=%fused_computation.5 | convolution fusion | flops 2150105088 | bytes 9437184 | tf_op jit(solution)/shard_map/senf,efd->send/dot_general | solution.py:40
  96.5 38.1 %all-to-all-done.2 = bf16[8,1,64,2048]{3,2,1,0:T(8,128)(2,1)} async-done(((bf16[8,1,64,2048]{3,2,1,0:T(8,128)(2,1)}), bf16[8,1,64,2048]{3,2,1,0:T(8,128)(2,1)}, u32[]{:S(2)}, u32[]{:S(2)}) %all-to-all-start.2) | async-done | bytes 2097184 | tf_op jit(solution)/shard_map/all_to_all | solution.py:36
  134.6 4.5 %fusion.31 = f32[8,1,64,512]{3,2,0,1:T(8,128)} fusion(bf16[1,2048,512]{2,1,0:T(8,128)(2,1)} %param.26, bf16[8,1,64,2048]{3,2,1,0:T(8,128)(2,1)} %all-to-all-done.2), kind=kOutput, calls=%fused_computation.24 | convolution fusion | flops 1073741824 | bytes 5242880 | tf_op jit(solution)/shard_map/send,edf->senf/dot_general | solution.py:37
  139.1 6.2 %fusion.1 = bf16[8,1,64,2048]{3,2,0,1:T(8,128)(2,1)} fusion(bf16[1,512,2048]{2,1,0:T(8,128)(2,1)S(1)} %copy-done, bf16[1,2048,512]{2,1,0:T(8,128)(2,1)} %param.27, bf16[8,1,64,2048]{3,2,1,0:T(8,128)(2,1)} %all-to-all-done.2, f32[8,1,64,512]{3,2,0,1:T(8,128)} %fusion.31), kind=kOutput, calls=%fused_computation.6 | convolution fusion | flops 2150105088 | bytes 9437184 | tf_op jit(solution)/shard_map/senf,efd->send/dot_general | solution.py:40
  146.5 1.6 convolution_convert_fusion.3
  148.1 1.4 collective-permute-start
  149.7 3.5 %all-to-all-start.1 = ((bf16[8,1,64,512]{3,2,1,0:T(8,128)(2,1)}), bf16[8,1,64,512]{3,2,1,0:T(8,128)(2,1)S(1)}, u32[]{:S(2)}, u32[]{:S(2)}) async-start(bf16[8,1,64,512]{3,2,1,0:T(8,128)(2,1)} %bitcast.165), calls=%async_computation.2 | async-start | bytes 1048576 | tf_op jit(solution)/shard_map/all_to_all | solution.py:42
  153.3 2.2 fusion.104
  156.0 13.6 %all_gather.7 = bf16[128,2048]{1,0:T(8,128)(2,1)} all-gather(bf16[128,512]{1,0:T(8,128)(2,1)S(1)} %fusion.66), channel_id=1, replica_groups=mesh['ep'=8,'tp'=4] {'tp'}, dimensions={1}, use_global_device_ids=true | all-gather | bytes 655360 | tf_op jit(solution)/shard_map/all_gather | solution.py:87
  169.7 11.3 %reduce-scatter.5.cloned.1.call-done = bf16[8,1,64,512]{3,2,0,1:T(8,128)(2,1)} async-done(((bf16[8,1,64,2048]{3,2,0,1:T(8,128)(2,1)}), bf16[8,1,64,512]{3,2,0,1:T(8,128)(2,1)}) %reduce-scatter.5.cloned.1.call-update) | async-done | bytes 524304 | tf_op jit(solution)/shard_map/reduce_scatter | solution.py:41
  181.0 4.6 %all-to-all-start.3 = ((bf16[8,1,64,512]{3,2,1,0:T(8,128)(2,1)}), bf16[8,1,64,512]{3,2,1,0:T(8,128)(2,1)}, u32[]{:S(2)}, u32[]{:S(2)}) async-start(bf16[8,1,64,512]{3,2,1,0:T(8,128)(2,1)} %bitcast.164), calls=%async_computation.5 | async-start | bytes 1048576 | tf_op jit(solution)/shard_map/all_to_all | solution.py:42
  185.9 8.9 %psum.7 = f32[128]{0:T(128)S(1)} all-reduce(f32[128]{0:T(128)S(1)} %get-tuple-element.2), channel_id=1, replica_groups=mesh['ep'=8,'tp'=4] {'tp'}, use_global_device_ids=true, to_apply=%region_2.3 | all-reduce | flops 128 | bytes 1024 | tf_op jit(solution)/shard_map/psum | solution.py:76
  195.0 10.2 %all_gather.6 = bf16[128,1024]{1,0:T(8,128)(2,1)S(1)} all-gather(bf16[128,256]{1,0:T(8,128)(2,1)S(1)} %multiply_convert_fusion), channel_id=1, replica_groups=mesh['ep'=8,'tp'=4] {'tp'}, dimensions={1}, use_global_device_ids=true | all-gather | bytes 327680 | tf_op jit(solution)/shard_map/all_gather | solution.py:86
  205.1 2.2 convolution_convert_fusion.2
  207.3 1.3 pad_maximum_fusion
  208.6 2.6 %gather_fusion.1 = bf16[512,512]{1,0:T(8,128)(2,1)} fusion(bf16[1024,512]{1,0:T(8,128)(2,1)S(1)} %bitcast.162, s32[1024]{0:T(1024)S(1)} %pad_clamp_fusion), kind=kCustom, calls=%fused_computation.1 | custom fusion | bytes 1050624 | tf_op jit(solution)/shard_map/gather | solution.py:115
  211.3 1.4 reshape.175
  213.4 2.9 %fusion.67 = bf16[128,512]{1,0:T(8,128)(2,1)} fusion(f32[128,512]{1,0:T(8,128)S(1)} %multiply_reduce_fusion, bf16[128,2048]{1,0:T(8,128)(2,1)} %all_gather.7, bf16[2048,512]{1,0:T(8,128)(2,1)} %param.31), kind=kOutput, calls=%fused_computation.38 | convolution fusion | flops 268566528 | bytes 3014656 | tf_op jit(solution)/shard_map/dot_general | solution.py:90
  (60 shorter events, 9.3 us)
Async XLA Ops:
  7.2 83.0 %copy-start = (bf16[1,512,2048]{2,1,0:T(8,128)(2,1)S(1)}, bf16[1,512,2048]{2,1,0:T(8,128)(2,1)}, u32[]{:S(2)}) copy-start(bf16[1,512,2048]{2,1,0:T(8,128)(2,1)} %param.28) | copy-start | bytes 6291460
  81.2 53.4 %all-to-all-start.2 = ((bf16[8,1,64,2048]{3,2,1,0:T(8,128)(2,1)}), bf16[8,1,64,2048]{3,2,1,0:T(8,128)(2,1)}, u32[]{:S(2)}, u32[]{:S(2)}) async-start(bf16[8,1,64,2048]{3,2,1,0:T(8,128)(2,1)} %get-tuple-element.5), calls=%async_computation.3 | async-start | bytes 4194304 | tf_op jit(solution)/shard_map/all_to_all | solution.py:36
  85.5 64.2 %reduce-scatter.3.cloned.1.call-start = ((), (), s32[]{:S(2)}) async-start(), calls=%async_computation.6 | async-start | bytes 2621440 | tf_op jit(solution)/shard_map/reduce_scatter | solution.py:41
  96.4 84.5 %reduce-scatter.5.cloned.1.call-start = ((), (), s32[]{:S(2)}) async-start(), calls=%async_computation.7 | async-start | bytes 2621440 | tf_op jit(solution)/shard_map/reduce_scatter | solution.py:41
  145.3 1.0 copy-start.2
  145.3 1.2 copy-start.7
  145.3 4.3 %copy-start.3 = (f32[128,4]{0,1:T(4,128)S(1)}, f32[128,4]{0,1:T(4,128)}, u32[]{:S(2)}) copy-start(f32[128,4]{0,1:T(4,128)} %param.25) | copy-start | bytes 6148
  148.1 21.6 %collective-permute-start = (bf16[15,256]{1,0:T(8,128)(2,1)S(1)}, bf16[15,256]{1,0:T(8,128)(2,1)S(1)}, u32[]{:S(2)}, u32[]{:S(2)}) collective-permute-start(bf16[15,256]{1,0:T(8,128)(2,1)S(1)} %slice.89), channel_id=1, source_target_pairs={{0,4},{4,8},{8,12},{12,16},{16,20},{20,24},{24,28},{1,5},{5,9},{9,... | collective-permute-start | bytes 23048 | tf_op jit(solution)/shard_map/ppermute | solution.py:14
  149.7 31.2 %all-to-all-start.1 = ((bf16[8,1,64,512]{3,2,1,0:T(8,128)(2,1)}), bf16[8,1,64,512]{3,2,1,0:T(8,128)(2,1)S(1)}, u32[]{:S(2)}, u32[]{:S(2)}) async-start(bf16[8,1,64,512]{3,2,1,0:T(8,128)(2,1)} %bitcast.165), calls=%async_computation.2 | async-start | bytes 1048576 | tf_op jit(solution)/shard_map/all_to_all | solution.py:42
  153.2 2.2 copy-start.6
  155.5 30.1 %copy-start.4 = (f32[256]{0:T(256)S(1)}, f32[256]{0:T(256)}, u32[]{:S(2)}) copy-start(f32[256]{0:T(256)} %param.21) | copy-start | bytes 3076
  156.0 38.9 %copy-start.5 = (f32[256]{0:T(256)S(1)}, f32[256]{0:T(256)}, u32[]{:S(2)}) copy-start(f32[256]{0:T(256)} %param.22) | copy-start | bytes 3076
  181.0 26.4 %copy-start.1 = (bf16[8,1,64,512]{3,2,1,0:T(8,128)(2,1)}, bf16[8,1,64,512]{3,2,1,0:T(8,128)(2,1)S(1)}, u32[]{:S(2)}) copy-start(bf16[8,1,64,512]{3,2,1,0:T(8,128)(2,1)S(1)} %all-to-all-done.1) | copy-start | bytes 1572868
  181.0 26.4 %all-to-all-start.3 = ((bf16[8,1,64,512]{3,2,1,0:T(8,128)(2,1)}), bf16[8,1,64,512]{3,2,1,0:T(8,128)(2,1)}, u32[]{:S(2)}, u32[]{:S(2)}) async-start(bf16[8,1,64,512]{3,2,1,0:T(8,128)(2,1)} %bitcast.164), calls=%async_computation.5 | async-start | bytes 1048576 | tf_op jit(solution)/shard_map/all_to_all | solution.py:42
Sparse Core Ops, SparseCore 0:
  96.6 36.4 reduce-scatter.2
  145.5 35.4 reduce-scatter.4
where the time goes:
time: 224 us; the launch traced here: 223 us
  blocking collectives  88 us (39%)
  waiting for transfers between devices  49.4 us (22%)
  matrix products  30.8 us (14%)
  local copies, waits for them, and re-layouts  19.4 us (9%)
  between operations  14.3 us (6%)
  starting transfers between devices  14 us (6%)
  other arithmetic  7.18 us (3%)
    all_to_all x1, blocking collectives, serve(): lax.all_to_all(sending, 'ep', split_axis=0, concat_axis=0, tiled=True)  55.3 us
    all_to_all x1, waiting for transfers between devices, serve(): lax.all_to_all(sending, 'ep', split_axis=0, concat_axis=0, tiled=True)  38.1 us
    all_gather x1, blocking collectives, on_device(): lax.all_gather(shared_hidden, 'tp', axis=1, tiled=True)  13.6 us
    dot_general x2, matrix products, serve(): jnp.einsum('senf,efd->send', hidden, expert_down, preferred_element_type=...  12.5 us
    reduce_scatter x2, waiting for transfers between devices, serve(): lax.psum_scatter(term.astype(jnp.bfloat16), 'tp', scatter_dimension=3, ti...  11.3 us
    all_gather x1, blocking collectives, on_device(): lax.all_gather(pooled_norm, 'tp', axis=1, tiled=True)  10.2 us
    dot_general x2, matrix products, serve(): jnp.einsum('send,edf->senf', arrived, expert_gate, preferred_element_type...  9.03 us
    psum x1, blocking collectives, on_device(): squares = lax.psum(jnp.sum(scaled * scaled, axis=1), 'tp')  8.92 us
  transfers between devices with their start and end apart: 6, of which 2 were waited for; matrix products, arithmetic and copies ran while one was open for 13% of the time, Pallas kernels for 0%

commit v1 on v0

--- a/solution.py
+++ b/solution.py
@@ -1,6 +1,8 @@
 import jax
 import jax.numpy as jnp
 from jax import lax
+from jax.experimental import pallas as pl
+from jax.experimental.pallas import tpu as pltpu
 from jax.sharding import PartitionSpec as P
 
 epsilon = 1e-06
@@ -119,9 +121,351 @@
     return (mix_out, moe_out)
 
 
+MESH = pl.DeviceIdType.MESH
+
+
+def places():
+    ep, tp = lax.axis_index("ep"), lax.axis_index("tp")
+    z, core = ep // 2, ep % 2
+    y, x = tp // 2, tp % 2
+    return ep, tp, z, core, y * 2 + 1 - x, (1 - y) * 2 + x, (1 - y) * 2 + 1 - x
+
+
+def greet(partners):
+    barrier = pltpu.get_barrier_semaphore()
+    for partner in partners:
+        pl.semaphore_signal(barrier, inc=1, device_id=partner, device_id_type=MESH)
+    pl.semaphore_wait(barrier, len(partners))
+
+
+def aligned(start, size):
+    return pl.ds(pl.multiple_of(start * size, size), size)
+
+
+def gather_kernel(n_ep, m_ref, w_ref, g_ref, wg_ref, *sems):
+    (w_s, w_r, z_s, z_r, x_s, x_r, y_s, y_r, dx_s, dx_r, dy_s, dy_r, c_s, c_r) = sems
+    ep, tp, z, core, xn, yn, _ = places()
+    n_z = n_ep // 2
+    rows = m_ref.shape[0]
+    cols = m_ref.shape[1] // 4
+    half = rows // 2
+    greet([((ep + m) % n_ep, tp) for m in range(1, n_ep)] + [(ep, xn), (ep, yn)])
+
+    def send(src, dst, s, r, device):
+        copy = pltpu.make_async_remote_copy(
+            src_ref=src, dst_ref=dst, send_sem=s, recv_sem=r, device_id=device, device_id_type=MESH
+        )
+        copy.start()
+        return copy
+
+    own_rows = aligned(ep, rows)
+    other_core = z * 2 + 1 - core
+    order = [k for k in (1, n_z - 1)] + list(range(2, n_z - 1))
+    z_copies = {}
+    for k in order:
+        target = ((z + k) % n_z) * 2 + core
+        z_copies[k] = send(
+            m_ref.at[:, aligned(tp, cols)],
+            g_ref.at[own_rows, aligned(tp, cols)],
+            z_s.at[k],
+            z_r.at[k],
+            (target, tp),
+        )
+    c_copies = {0: send(m_ref, g_ref.at[own_rows, :], c_s.at[0], c_r.at[0], (other_core, tp))}
+    w_copies = [
+        send(w_ref, wg_ref.at[ep], w_s.at[m], w_r.at[m], ((ep + m) % n_ep, tp))
+        for m in range(1, n_ep)
+    ]
+    g_ref[own_rows, :] = m_ref[...]
+    wg_ref[ep] = w_ref[...]
+    x_copies, y_copies, dx_copies, dy_copies = {}, {}, {}, {}
+
+    def block(k):
+        return ((z + n_z - k) % n_z) * 2 + core
+
+    def piece(k, quarter):
+        return g_ref.at[aligned(block(k), rows), aligned(quarter, cols)]
+
+    def half_piece(k, part, quarter):
+        start = pl.multiple_of(block(k) * rows + part * half, half)
+        return g_ref.at[pl.ds(start, half), aligned(quarter, cols)]
+
+    def across(k):
+        z_copies[k].wait_recv()
+        x_copies[k] = send(piece(k, tp), piece(k, tp), x_s.at[k], x_r.at[k], (ep, xn))
+        y_copies[k] = send(piece(k, tp), piece(k, tp), y_s.at[k], y_r.at[k], (ep, yn))
+
+    def corner(k):
+        x_copies[k].wait_recv()
+        dx_copies[k] = send(
+            half_piece(k, 0, xn), half_piece(k, 0, xn), dx_s.at[k], dx_r.at[k], (ep, yn)
+        )
+        y_copies[k].wait_recv()
+        dy_copies[k] = send(
+            half_piece(k, 1, yn), half_piece(k, 1, yn), dy_s.at[k], dy_r.at[k], (ep, xn)
+        )
+
+    def over(k):
+        dx_copies[k].wait_recv()
+        dy_copies[k].wait_recv()
+        whole = g_ref.at[aligned(block(k), rows), :]
+        c_copies[k] = send(whole, whole, c_s.at[k], c_r.at[k], (other_core, tp))
+
+    for index in range(len(order) + 2):
+        if index < len(order):
+            across(order[index])
+        if 1 <= index < len(order) + 1:
+            corner(order[index - 1])
+        if index >= 2:
+            over(order[index - 2])
+    for k in [0] + order:
+        c_copies[k].wait_recv()
+    for copy in w_copies:
+        copy.wait()
+    for group in (z_copies, x_copies, y_copies, dx_copies, dy_copies, c_copies):
+        for copy in group.values():
+            copy.wait_send()
+
+
+def gather_rows(moe_norm, dense, n_ep):
+    n_z = n_ep // 2
+    sems = [pltpu.SemaphoreType.DMA((n_ep,))] * 2 + [pltpu.SemaphoreType.DMA((n_z,))] * 12
+    vmem = pl.BlockSpec(memory_space=pltpu.VMEM)
+    return pl.pallas_call(
+        lambda *refs: gather_kernel(n_ep, *refs),
+        out_shape=(
+            jax.ShapeDtypeStruct((n_ep * moe_norm.shape[0], moe_norm.shape[1]), jnp.bfloat16),
+            jax.ShapeDtypeStruct((n_ep,) + dense.shape, jnp.float32),
+        ),
+        in_specs=[vmem] * 2,
+        out_specs=(vmem, vmem),
+        scratch_shapes=sems,
+        compiler_params=pltpu.CompilerParams(collective_id=0, has_side_effects=True),
+    )(moe_norm, dense)
+
+
+def reduce_kernel(n_ep, p_ref, sh_ref, po_ref, sq_ref, o_ref, sh_all, po_all, sq_all, *scratch):
+    (ca, s, bx, by, qx, qy, r, bz) = scratch[:8]
+    (c_s, c_r, dx_s, dx_r, dy_s, dy_r, x_s, x_r, y_s, y_r, z_s, z_r, t_s, t_r) = scratch[8:]
+    ep, tp, z, core, xn, yn, dg = places()
+    n_z = n_ep // 2
+    rows = o_ref.shape[0]
+    cols = o_ref.shape[1]
+    half = rows // 2
+    other_core = z * 2 + 1 - core
+    peers = (xn, yn, dg)
+    greet(
+        [(other_core, tp)]
+        + [(((z + k) % n_z) * 2 + core, tp) for k in range(1, n_z)]
+        + [(ep, t) for t in peers]
+    )
+
+    def send(src, dst, sem_s, sem_r, device):
+        copy = pltpu.make_async_remote_copy(
+            src_ref=src, dst_ref=dst, send_sem=sem_s, recv_sem=sem_r, device_id=device, device_id_type=MESH
+        )
+        copy.start()
+        return copy
+
+    order = list(range(2, n_z - 1)) + [1, n_z - 1, 0]
+    c_copies, dx_copies, dy_copies, x_copies, y_copies, z_copies = {}, {}, {}, {}, {}, {}
+    for k in order:
+        away = ((z + k) % n_z) * 2 + 1 - core
+        c_copies[k] = send(
+            p_ref.at[aligned(away, rows), :], ca.at[k], c_s.at[k], c_r.at[k], (other_core, tp)
+        )
+    low, high = pl.ds(0, half), pl.ds(half, half)
+
+    def first(k):
+        c_copies[k].wait_recv()
+        mine = ((z + k) % n_z) * 2 + core
+        s[k] = (
+            p_ref[aligned(mine, rows), :].astype(jnp.float32) + ca[k].astype(jnp.float32)
+        ).astype(jnp.bfloat16)
+        dx_copies[k] = send(
+            s.at[k, low, aligned(dg, cols)], bx.at[k], dx_s.at[k], dx_r.at[k], (ep, xn)
+        )
+        dy_copies[k] = send(
+            s.at[k, high, aligned(dg, cols)], by.at[k], dy_s.at[k], dy_r.at[k], (ep, yn)
+        )
+
+    def second(k):
+        dx_copies[k].wait_recv()
+        s[k, low, aligned(yn, cols)] = (
+            s[k, low, aligned(yn, cols)].astype(jnp.float32) + bx[k].astype(jnp.float32)
+        ).astype(jnp.bfloat16)
+        y_copies[k] = send(
+            s.at[k, :, aligned(yn, cols)], qy.at[k], y_s.at[k], y_r.at[k], (ep, yn)
+        )
+        dy_copies[k].wait_recv()
+        s[k, high, aligned(xn, cols)] = (
+            s[k, high, aligned(xn, cols)].astype(jnp.float32) + by[k].astype(jnp.float32)
+        ).astype(jnp.bfloat16)
+        x_copies[k] = send(
+            s.at[k, :, aligned(xn, cols)], qx.at[k], x_s.at[k], x_r.at[k], (ep, xn)
+        )
+
+    def third(k):
+        x_copies[k].wait_recv()
+        y_copies[k].wait_recv()
+        total = (
+            s[k, :, aligned(tp, cols)].astype(jnp.float32)
+            + qx[k].astype(jnp.float32)
+            + qy[k].astype(jnp.float32)
+        )
+        if k == 0:
+            o_ref[...] = total
+        else:
+            r[k] = total.astype(jnp.bfloat16)
+            target = ((z + k) % n_z) * 2 + core
+            z_copies[k] = send(r.at[k], bz.at[k], z_s.at[k], z_r.at[k], (target, tp))
+
+    t_copies = []
+    for index in range(n_z + 2):
+        if index < n_z:
+            first(order[index])
+        if 1 <= index < n_z + 1:
+            second(order[index - 1])
+        if index == n_z:
+            for number, t in enumerate(peers):
+                pairs = (
+                    (sh_ref, sh_all.at[:, aligned(tp, sh_ref.shape[1])]),
+                    (po_ref, po_all.at[:, aligned(tp, po_ref.shape[1])]),
+                    (sq_ref, sq_all.at[tp]),
+                )
+                for kind, (src, dst) in enumerate(pairs):
+                    t_copies.append(
+                        send(src, dst, t_s.at[number, kind], t_r.at[number, kind], (ep, t))
+                    )
+        if index >= 2:
+            third(order[index - 2])
+    sh_all[:, aligned(tp, sh_ref.shape[1])] = sh_ref[...]
+    po_all[:, aligned(tp, po_ref.shape[1])] = po_ref[...]
+    sq_all[tp] = sq_ref[...]
+    for k in order[:-1]:
+        z_copies[k].wait_recv()
+        o_ref[...] += bz[k].astype(jnp.float32)
+    for copy in t_copies:
+        copy.wait()
+    for group in (c_copies, dx_copies, dy_copies, x_copies, y_copies, z_copies):
+        for copy in group.values():
+            copy.wait_send()
+
+
+def reduce_rows(weighted, shared_hidden, pooled, squares, n_ep, n_tp):
+    n_z = n_ep // 2
+    rows, width = weighted.shape[0] // n_ep, weighted.shape[1]
+    cols = width // n_tp
+    half = rows // 2
+    bf16 = jnp.bfloat16
+    vmem = pl.BlockSpec(memory_space=pltpu.VMEM)
+    scratch = [
+        pltpu.VMEM((n_z, rows, width), bf16),
+        pltpu.VMEM((n_z, rows, width), bf16),
+        pltpu.VMEM((n_z, half, cols), bf16),
+        pltpu.VMEM((n_z, half, cols), bf16),
+        pltpu.VMEM((n_z, rows, cols), bf16),
+        pltpu.VMEM((n_z, rows, cols), bf16),
+        pltpu.VMEM((n_z, rows, cols), bf16),
+        pltpu.VMEM((n_z, rows, cols), bf16),
+    ]
+    sems = [pltpu.SemaphoreType.DMA((n_z,))] * 12 + [pltpu.SemaphoreType.DMA((3, 3))] * 2
+    return pl.pallas_call(
+        lambda *refs: reduce_kernel(n_ep, *refs),
+        out_shape=(
+            jax.ShapeDtypeStruct((rows, cols), jnp.float32),
+            jax.ShapeDtypeStruct((rows, n_tp * shared_hidden.shape[1]), bf16),
+            jax.ShapeDtypeStruct((rows, n_tp * pooled.shape[1]), bf16),
+            jax.ShapeDtypeStruct((n_tp,) + squares.shape, jnp.float32),
+        ),
+        in_specs=[vmem] * 4,
+        out_specs=(vmem,) * 4,
+        scratch_shapes=scratch + sems,
+        compiler_params=pltpu.CompilerParams(
+            collective_id=1, has_side_effects=True, vmem_limit_bytes=40 << 20
+        ),
+    )(weighted, shared_hidden, pooled, squares)
+
+
+def dense_on_device(
+    mix_input,
+    expert_input,
+    mix_gain,
+    moe_gain,
+    pool_in,
+    pool_scale,
+    pool_gain,
+    pool_out,
+    route,
+    route_score,
+    expert_gate,
+    expert_up,
+    expert_down,
+    shared_gate,
+    shared_up,
+    shared_down,
+):
+    n_ep, n_tp = lax.axis_size("ep"), lax.axis_size("tp")
+    me = lax.axis_index("ep")
+    tok_rows = mix_input.shape[0]
+    channels = pool_in.shape[1]
+    pool_width = channels * n_tp
+    f32 = jnp.float32
+
+    moe_norm = row_norm(expert_input, moe_gain)
+    weights = 2.5 * route_score / jnp.sum(route_score, axis=1, keepdims=True)
+    experts = jnp.arange(n_ep, dtype=jnp.int32)
+    dense = jnp.sum(
+        jnp.where(route.T[None, :, :] == experts[:, None, None], weights.T[None, :, :], 0.0), axis=1
+    )
+    mix_norm = row_norm(mix_input, mix_gain)
+    pool_input = jnp.dot(mix_norm, pool_in, preferred_element_type=f32).astype(jnp.bfloat16)
+    before = shifted(pool_input[tok_rows - reach_rows :], "ep", 1)
+    all_rows, all_weights = gather_rows(moe_norm, dense, n_ep)
+
+    extended = jnp.concatenate([before, pool_input], axis=0).astype(f32)
+    position = (me * tok_rows + jnp.arange(tok_rows, dtype=jnp.int32) + 1).astype(f32)
+    channel_ids = lax.axis_index("tp") * channels + jnp.arange(channels, dtype=jnp.int32)
+    group = channel_ids // (pool_width // 4)
+    scaled = window_means(extended, position, group, tok_rows) * pool_scale
+    squares = jnp.sum(scaled * scaled, axis=1)[None, :]
+    pooled = (scaled * pool_gain).astype(jnp.bfloat16)
+    shared_hidden = (
+        jax.nn.silu(jnp.dot(moe_norm, shared_gate, preferred_element_type=f32))
+        * jnp.dot(moe_norm, shared_up, preferred_element_type=f32)
+    ).astype(jnp.bfloat16)
+
+    factor = lax.dynamic_index_in_dim(all_weights, me, axis=1, keepdims=False).reshape(-1, 1)
+    gate = jnp.dot(all_rows, expert_gate[0], preferred_element_type=f32)
+    upper = jnp.dot(all_rows, expert_up[0], preferred_element_type=f32)
+    hidden = (jax.nn.silu(gate) * upper).astype(jnp.bfloat16)
+    weighted = (jnp.dot(hidden, expert_down[0], preferred_element_type=f32) * factor).astype(
+        jnp.bfloat16
+    )
+    routed, shared_all, pooled_all, squares_all = reduce_rows(
+        weighted, shared_hidden, pooled, squares, n_ep, n_tp
+    )
+    mean = jnp.sum(squares_all, axis=0).reshape(-1, 1) / pool_width
+    mix_out = (
+        jnp.dot(pooled_all, pool_out, preferred_element_type=f32) * lax.rsqrt(mean + epsilon)
+    ).astype(jnp.bfloat16)
+    shared_part = jnp.dot(shared_all, shared_down, preferred_element_type=f32)
+    return (mix_out, (routed + shared_part).astype(jnp.bfloat16))
+
+
+def chosen(*arrays):
+    route, expert_gate = arrays[8], arrays[10]
+    experts = expert_gate.shape[0] * lax.axis_size("ep")
+    capacity = 2 * route.shape[0] * route.shape[1] // experts
+    square = lax.axis_size("tp") == 4 and lax.axis_size("ep") >= 6
+    if capacity == route.shape[0] and expert_gate.shape[0] == 1 and square:
+        return dense_on_device(*arrays)
+    return on_device(*arrays)
+
+
 def solution(mesh):
     return jax.shard_map(
-        on_device,
+        chosen,
         mesh=mesh,
         in_specs=(
             P("ep", None),

time: 224 us -> 103 us (0.46)
  blocking collectives: 88 us -> 0 us
  Pallas kernels: 0 us -> 65.5 us
  waiting for transfers between devices: 49.4 us -> 0.01 us
  local copies, waits for them, and re-layouts: 19.4 us -> 3.29 us
  between operations: 14.3 us -> 0.85 us
  starting transfers between devices: 14 us -> 2.4 us
  other arithmetic: 7.18 us -> 2.83 us
  matrix products: 30.8 us -> 27.3 us
    pallas_call x0 -> x2, Pallas kernels: none -> 65.5 us  [the longest x1 33.2 us: reduce_rows(): pl.pallas_call(lambda *refs: reduce_kernel(n_ep, *refs), out_shape=(jax.S...]
    all_to_all x1 -> x0, blocking collectives: 55.3 us -> none  [serve(): lax.all_to_all(sending, 'ep', split_axis=0, concat_axis=0, tiled=True)]
    all_to_all x3 -> x0, waiting for transfers between devices: 38.1 us -> none  [the longest x1 38.1 us: serve(): lax.all_to_all(sending, 'ep', split_axis=0, concat_axis=0, tiled=True)]
    all_gather x2 -> x0, blocking collectives: 23.8 us -> none  [the longest x1 13.6 us: on_device(): lax.all_gather(shared_hidden, 'tp', axis=1, tiled=True)]
    all_to_all x3 -> x0, starting transfers between devices: 12.5 us -> none  [the longest x2 8.12 us: serve(): return lax.all_to_all(summed, 'ep', split_axis=0, concat_axis=0, tiled=True)]
    reduce_scatter x2 -> x0, waiting for transfers between devices: 11.3 us -> none  [serve(): lax.psum_scatter(term.astype(jnp.bfloat16), 'tp', scatter_dimension=3, ti...]
    psum x1 -> x0, blocking collectives: 8.92 us -> none  [on_device(): squares = lax.psum(jnp.sum(scaled * scaled, axis=1), 'tp')]
    gather x2 -> x0, local copies, waits for them, and re-layouts: 8.64 us -> none  [the longest x1 6.02 us: on_device(): padded_rows[owner]]
  transfers between devices with their start and end apart: 6 -> 1, of which waited for: 2 -> 0; matrix products, arithmetic and copies ran while one was open for 13% -> 22% of each run, Pallas kernels for 0% -> 32%
where the time goes in v1:
time: 103 us; the launch traced here: 102 us
  Pallas kernels  65.5 us (64%)
  matrix products  27.3 us (27%)
  local copies, waits for them, and re-layouts  3.29 us (3%)
  other arithmetic  2.83 us (3%)
  starting transfers between devices  2.4 us (2%)
    pallas_call x1, Pallas kernels, reduce_rows(): pl.pallas_call(lambda *refs: reduce_kernel(n_ep, *refs), out_shape=(jax.S...  33.2 us
    pallas_call x1, Pallas kernels, gather_rows(): pl.pallas_call(lambda *refs: gather_kernel(n_ep, *refs), out_shape=(jax.S...  32.3 us
    dot_general x1, matrix products, dense_on_device(): jnp.dot(hidden, expert_down[0], preferred_element_type=f32) * factor  10.1 us
    dot_general x1, matrix products, dense_on_device(): upper = jnp.dot(all_rows, expert_up[0], preferred_element_type=f32)  5.9 us
    dot_general x1, matrix products, dense_on_device(): shared_part = jnp.dot(shared_all, shared_down, preferred_element_type=f32)  2.7 us
    unnamed x20, local copies, waits for them, and re-layouts  2.52 us
    ppermute x1, starting transfers between devices, shifted(): return lax.ppermute(block, axis, route)  2.4 us
    dot_general x1, matrix products, dense_on_device(): jnp.dot(moe_norm, shared_up, preferred_element_type=f32)  2.36 us
  transfers between devices with their start and end apart: 1, of which 0 were waited for; matrix products, arithmetic and copies ran while one was open for 22% of the time, Pallas kernels for 32%

profile of v1, /device:TPU:0, one launch (start us, length us, event | category | flops | bytes accessed | tf_op | source)
XLA Modules:
  0.0 102.1 jit_solution(17680259560320953809)
XLA Ops:
  0.6 0.0 copy-start
  0.7 1.4 %fusion.13 = f32[128]{0:T(128)S(1)} fusion(bf16[128,2048]{1,0:T(8,128)(2,1)} %param.16), kind=kLoop, calls=%fused_computation.21 | loop fusion | flops 786304 | bytes 524800 | tf_op jit(solution)/shard_map/reduce_sum | solution.py:21
  2.1 1.8 %convolution_convert_fusion = bf16[128,256]{1,0:T(8,128)(2,1)S(1)} fusion(bf16[2048,256]{1,0:T(8,128)(2,1)} %param.20, bf16[128,2048]{1,0:T(8,128)(2,1)} %param.16, f32[2048]{0:T(1024)} %param.18, f32[128]{0:T(128)S(1)} %add_rsqrt_fusion.1), kind=kOutput, calls=%fused_computation.17 | convolution fusion | flops 135299072 | bytes 1647104 | tf_op jit(solution)/shard_map/dot_general | solution.py:422
  3.9 2.4 %collective-permute-start = (bf16[15,256]{1,0:T(8,128)(2,1)S(1)}, bf16[15,256]{1,0:T(8,128)(2,1)S(1)}, u32[]{:S(2)}, u32[]{:S(2)}) collective-permute-start(bf16[15,256]{1,0:T(8,128)(2,1)S(1)} %slice.69), channel_id=1, source_target_pairs={{0,4},{4,8},{8,12},{12,16},{16,20},{20,24},{24,28},{1,5},{5,9},{9,... | collective-permute-start | bytes 23048 | tf_op jit(solution)/shard_map/ppermute | solution.py:16
  6.3 0.0 copy-done.3
  6.3 0.2 fusion.10
  6.6 0.0 copy-done.6
  6.6 0.6 select_reduce_fusion.refs_1_
  7.2 0.0 copy-done.4
  7.2 0.2 fusion.12.refs_0_
  7.4 2.2 %fusion.27 = f32[128,512]{1,0:T(8,128)S(1)} fusion(bf16[128,2048]{1,0:T(8,128)(2,1)S(1)} %fusion.12.refs_0_, bf16[2048,512]{1,0:T(8,128)(2,1)} %param.29), kind=kOutput, calls=%fused_computation.69 | convolution fusion | flops 268435456 | bytes 2883584 | tf_op jit(solution)/shard_map/dot_general | solution.py:434
  9.6 32.3 %shard_map.167 = (bf16[1024,2048]{1,0:T(8,128)(2,1)}, f32[8,8,128]{2,1,0:T(8,128)}) custom-call(bf16[128,2048]{1,0:T(8,128)(2,1)} %copy-done.2, f32[8,128]{1,0:T(8,128)} %select_reduce_fusion.refs_1_), custom_call_target="tpu_custom_call" | custom-call | tf_op jit(solution)/shard_map/pallas_call | solution.py:234
  42.0 0.0 copy-start.9
  42.0 2.4 %fusion.7.refs_1_ = bf16[128,512]{1,0:T(8,128)(2,1)S(1)} fusion(bf16[128,2048]{1,0:T(8,128)(2,1)} %copy-done.2, bf16[2048,512]{1,0:T(8,128)(2,1)} %param.30, f32[128,512]{1,0:T(8,128)S(1)} %fusion.27), kind=kOutput, calls=%fused_computation.14 | convolution fusion | flops 268828672 | bytes 3014656 | tf_op jit(solution)/shard_map/dot_general | solution.py:435
  44.4 0.8 constant_dynamic-slice_fusion
  45.1 5.9 %fusion.1 = f32[1024,512]{1,0:T(8,128)} fusion(bf16[1024,2048]{1,0:T(8,128)(2,1)} %get-tuple-element.8, bf16[1,2048,512]{2,1,0:T(8,128)(2,1)S(1)} %copy-done.9), kind=kOutput, calls=%fused_computation.2 | convolution fusion | flops 2147483648 | bytes 8388608 | tf_op jit(solution)/shard_map/dot_general | solution.py:440
  51.0 10.1 %multiply_convert_fusion.refs_0_ = bf16[1024,2048]{1,0:T(8,128)(2,1)} fusion(f32[1024]{0:T(1024)S(1)} %bitcast.30, bf16[1,512,2048]{2,1,0:T(8,128)(2,1)S(1)} %copy-done, f32[1024,512]{1,0:T(8,128)} %fusion.1, bf16[1024,2048]{1,0:T(8,128)(2,1)} %get-tuple-element.8, bf16[1,2048,512]{2,1,0:T(8,128)(2,1)} %param.26), kind=kOutput, calls=%fused_computation | convolution fusion | flops 4302307328 | bytes 14684160 | tf_op jit(solution)/shard_map/dot_general | solution.py:442
  61.2 0.0 collective-permute-done
  61.2 0.3 multiply_reduce_fusion
  61.5 0.3 copy-done.8
  61.8 2.2 %copy-done.1 = bf16[1024,2048]{1,0:T(8,128)(2,1)S(1)} copy-done((bf16[1024,2048]{1,0:T(8,128)(2,1)S(1)}, bf16[1024,2048]{1,0:T(8,128)(2,1)}, u32[]{:S(2)}) %copy-start.1) | copy-done | bytes 4194328
  64.0 33.2 %shard_map.168 = (f32[128,512]{1,0:T(8,128)S(1)}, bf16[128,2048]{1,0:T(8,128)(2,1)S(1)}, bf16[128,1024]{1,0:T(8,128)(2,1)S(1)}, f32[4,1,128]{2,1,0:T(1,128)S(1)}) custom-call(bf16[1024,2048]{1,0:T(8,128)(2,1)S(1)} %copy-done.1, bf16[128,512]{1,0:T(8,128)(2,1)S(1)} %fusion.7.refs_1_, bf16[128,256]{1,0:T(8,128)(2,1)S(1)} %multiply_convert_fusion.2.refs_2_, ...), custom_call_target="tpu_custom_call" | custom-call | tf_op jit(solution)/shard_map/pallas_call | solution.py:373
  97.2 2.2 %fusion.9 = bf16[128,512]{1,0:T(8,128)(2,1)} fusion(bf16[128,1024]{1,0:T(8,128)(2,1)S(1)} %get-tuple-element.10, bf16[1024,512]{1,0:T(8,128)(2,1)} %param.23, f32[128]{0:T(128)S(1)} %add_rsqrt_fusion), kind=kOutput, calls=%fused_computation.16 | convolution fusion | flops 134348800 | bytes 1442304 | tf_op jit(solution)/shard_map/dot_general | solution.py:450
  99.4 2.7 %fusion.8 = bf16[128,512]{1,0:T(8,128)(2,1)} fusion(f32[128,512]{1,0:T(8,128)S(1)} %get-tuple-element.12, bf16[128,2048]{1,0:T(8,128)(2,1)S(1)} %get-tuple-element.13, bf16[2048,512]{1,0:T(8,128)(2,1)} %param.31), kind=kOutput, calls=%fused_computation.15 | convolution fusion | flops 268566528 | bytes 3014656 | tf_op jit(solution)/shard_map/dot_general | solution.py:452
  (26 shorter events, 0.2 us)
Async XLA Ops:
  0.6 50.4 %copy-start = (bf16[1,512,2048]{2,1,0:T(8,128)(2,1)S(1)}, bf16[1,512,2048]{2,1,0:T(8,128)(2,1)}, u32[]{:S(2)}) copy-start(bf16[1,512,2048]{2,1,0:T(8,128)(2,1)} %param.28) | copy-start | bytes 6291460
  0.6 5.6 %copy-start.3 = (bf16[128,2048]{1,0:T(8,128)(2,1)S(1)}, bf16[128,2048]{1,0:T(8,128)(2,1)}, u32[]{:S(2)}) copy-start(bf16[128,2048]{1,0:T(8,128)(2,1)} %param.17) | copy-start | bytes 1572868
  0.7 5.9 %copy-start.5 = (f32[128,4]{0,1:T(4,128)S(1)}, f32[128,4]{0,1:T(4,128)}, u32[]{:S(2)}) copy-start(f32[128,4]{0,1:T(4,128)} %param.25) | copy-start | bytes 6148
  0.7 5.9 %copy-start.6 = (s32[128,4]{0,1:T(4,128)S(1)}, s32[128,4]{0,1:T(4,128)}, u32[]{:S(2)}) copy-start(s32[128,4]{0,1:T(4,128)} %param.24) | copy-start | bytes 6148
  0.7 6.5 %copy-start.4 = (f32[2048]{0:T(1024)S(1)}, f32[2048]{0:T(1024)}, u32[]{:S(2)}) copy-start(f32[2048]{0:T(1024)} %param.19) | copy-start | bytes 24580
  3.9 57.3 %collective-permute-start = (bf16[15,256]{1,0:T(8,128)(2,1)S(1)}, bf16[15,256]{1,0:T(8,128)(2,1)S(1)}, u32[]{:S(2)}, u32[]{:S(2)}) collective-permute-start(bf16[15,256]{1,0:T(8,128)(2,1)S(1)} %slice.69), channel_id=1, source_target_pairs={{0,4},{4,8},{8,12},{12,16},{16,20},{20,24},{24,28},{1,5},{5,9},{9,... | collective-permute-start | bytes 23048 | tf_op jit(solution)/shard_map/ppermute | solution.py:16
  7.4 2.3 %copy-start.2 = (bf16[128,2048]{1,0:T(8,128)(2,1)}, bf16[128,2048]{1,0:T(8,128)(2,1)S(1)}, u32[]{:S(2)}) copy-start(bf16[128,2048]{1,0:T(8,128)(2,1)S(1)} %fusion.12.refs_0_) | copy-start | bytes 1572868
  42.0 3.1 %copy-start.9 = (bf16[1,2048,512]{2,1,0:T(8,128)(2,1)S(1)}, bf16[1,2048,512]{2,1,0:T(8,128)(2,1)}, u32[]{:S(2)}) copy-start(bf16[1,2048,512]{2,1,0:T(8,128)(2,1)} %param.27) | copy-start | bytes 6291460
  51.0 10.2 %copy-start.7 = (f32[256]{0:T(256)S(1)}, f32[256]{0:T(256)}, u32[]{:S(2)}) copy-start(f32[256]{0:T(256)} %param.21) | copy-start | bytes 3076
  61.1 0.7 copy-start.8
  61.8 2.2 %copy-start.1 = (bf16[1024,2048]{1,0:T(8,128)(2,1)S(1)}, bf16[1024,2048]{1,0:T(8,128)(2,1)}, u32[]{:S(2)}) copy-start(bf16[1024,2048]{1,0:T(8,128)(2,1)} %multiply_convert_fusion.refs_0_) | copy-start | bytes 12582916

commit v2 on v1

--- a/solution.py
+++ b/solution.py
@@ -240,7 +240,7 @@
         in_specs=[vmem] * 2,
         out_specs=(vmem, vmem),
         scratch_shapes=sems,
-        compiler_params=pltpu.CompilerParams(collective_id=0, has_side_effects=True),
+        compiler_params=pltpu.CompilerParams(collective_id=0, has_side_effects=True, vmem_limit_bytes=16 << 20),
     )(moe_norm, dense)
 
 
@@ -382,7 +382,7 @@
         out_specs=(vmem,) * 4,
         scratch_shapes=scratch + sems,
         compiler_params=pltpu.CompilerParams(
-            collective_id=1, has_side_effects=True, vmem_limit_bytes=40 << 20
+            collective_id=1, has_side_effects=True, vmem_limit_bytes=16 << 20
         ),
     )(weighted, shared_hidden, pooled, squares)
 
@@ -438,10 +438,8 @@
     factor = lax.dynamic_index_in_dim(all_weights, me, axis=1, keepdims=False).reshape(-1, 1)
     gate = jnp.dot(all_rows, expert_gate[0], preferred_element_type=f32)
     upper = jnp.dot(all_rows, expert_up[0], preferred_element_type=f32)
-    hidden = (jax.nn.silu(gate) * upper).astype(jnp.bfloat16)
-    weighted = (jnp.dot(hidden, expert_down[0], preferred_element_type=f32) * factor).astype(
-        jnp.bfloat16
-    )
+    hidden = (jax.nn.silu(gate) * upper * factor).astype(jnp.bfloat16)
+    weighted = jnp.dot(hidden, expert_down[0], preferred_element_type=f32).astype(jnp.bfloat16)
     routed, shared_all, pooled_all, squares_all = reduce_rows(
         weighted, shared_hidden, pooled, squares, n_ep, n_tp
     )

time: 103 us -> 99.8 us (0.969)
  Pallas kernels: 65.5 us -> 62.6 us
  local copies, waits for them, and re-layouts: 3.29 us -> 4.46 us
    pallas_call x1, Pallas kernels: 32.3 us -> 29.5 us  [gather_rows(): pl.pallas_call(lambda *refs: gather_kernel(n_ep, *refs), out_shape=(jax.S...]
    unnamed x20, local copies, waits for them, and re-layouts: 2.52 us -> 4.44 us
  transfers between devices with their start and end apart: 1 -> 1, of which waited for: 0 -> 0; matrix products, arithmetic and copies ran while one was open for 22% -> 21% of each run, Pallas kernels for 32% -> 30%
where the time goes in v2:
time: 99.8 us; the launch traced here: 99.5 us
  Pallas kernels  62.6 us (63%)
  matrix products  26.9 us (27%)
  local copies, waits for them, and re-layouts  4.46 us (4%)
  starting transfers between devices  2.4 us (2%)
  other arithmetic  2.24 us (2%)
    pallas_call x1, Pallas kernels, reduce_rows(): pl.pallas_call(lambda *refs: reduce_kernel(n_ep, *refs), out_shape=(jax.S...  33.1 us
    pallas_call x1, Pallas kernels, gather_rows(): pl.pallas_call(lambda *refs: gather_kernel(n_ep, *refs), out_shape=(jax.S...  29.5 us
    dot_general x1, matrix products, dense_on_device(): jnp.dot(hidden, expert_down[0], preferred_element_type=f32)  10.1 us
    dot_general x1, matrix products, dense_on_device(): upper = jnp.dot(all_rows, expert_up[0], preferred_element_type=f32)  5.91 us
    unnamed x20, local copies, waits for them, and re-layouts  4.44 us
    dot_general x1, matrix products, dense_on_device(): shared_part = jnp.dot(shared_all, shared_down, preferred_element_type=f32)  2.7 us
    ppermute x1, starting transfers between devices, shifted(): return lax.ppermute(block, axis, route)  2.4 us
    dot_general x1, matrix products, dense_on_device(): jnp.dot(pooled_all, pool_out, preferred_element_type=f32)  2.2 us
  transfers between devices with their start and end apart: 1, of which 0 were waited for; matrix products, arithmetic and copies ran while one was open for 21% of the time, Pallas kernels for 30%

profile of v2, /device:TPU:0, one launch (start us, length us, event | category | flops | bytes accessed | tf_op | source)
XLA Modules:
  0.0 99.5 jit_solution(14325465043757703297)
XLA Ops:
  0.6 0.0 copy-start
  0.6 0.0 copy-start.3
  0.7 0.0 copy-start.5
  0.7 1.4 %fusion.13 = f32[128]{0:T(128)S(1)} fusion(bf16[128,2048]{1,0:T(8,128)(2,1)} %param.16), kind=kLoop, calls=%fused_computation.21 | loop fusion | flops 786304 | bytes 524800 | tf_op jit(solution)/shard_map/reduce_sum | solution.py:21
  2.1 1.8 %convolution_convert_fusion.1 = bf16[128,256]{1,0:T(8,128)(2,1)S(1)} fusion(bf16[2048,256]{1,0:T(8,128)(2,1)} %param.20, bf16[128,2048]{1,0:T(8,128)(2,1)} %param.16, f32[2048]{0:T(1024)} %param.18, f32[128]{0:T(128)S(1)} %add_rsqrt_fusion.1), kind=kOutput, calls=%fused_computation.17 | convolution fusion | flops 135299072 | bytes 1647104 | tf_op jit(solution)/shard_map/dot_general | solution.py:422
  3.9 2.4 %collective-permute-start = (bf16[15,256]{1,0:T(8,128)(2,1)S(1)}, bf16[15,256]{1,0:T(8,128)(2,1)S(1)}, u32[]{:S(2)}, u32[]{:S(2)}) collective-permute-start(bf16[15,256]{1,0:T(8,128)(2,1)S(1)} %slice.69), channel_id=1, source_target_pairs={{0,4},{4,8},{8,12},{12,16},{16,20},{20,24},{24,28},{1,5},{5,9},{9,... | collective-permute-start | bytes 23048 | tf_op jit(solution)/shard_map/ppermute | solution.py:16
  6.3 0.2 fusion.10
  6.5 0.0 copy-done.5
  6.6 0.2 fusion.12.refs_0_
  6.8 2.0 %fusion.27 = f32[128,512]{1,0:T(8,128)S(1)} fusion(bf16[128,2048]{1,0:T(8,128)(2,1)S(1)} %fusion.12.refs_0_, bf16[2048,512]{1,0:T(8,128)(2,1)} %param.29), kind=kOutput, calls=%fused_computation.69 | convolution fusion | flops 268435456 | bytes 2883584 | tf_op jit(solution)/shard_map/dot_general | solution.py:434
  8.8 29.5 %shard_map.167 = (bf16[1024,2048]{1,0:T(8,128)(2,1)S(1)}, f32[8,8,128]{2,1,0:T(8,128)S(1)}) custom-call(bf16[128,2048]{1,0:T(8,128)(2,1)S(1)} %fusion.12.refs_0_, f32[8,128]{1,0:T(8,128)S(1)} %select_reduce_fusion.refs_1_), custom_call_target="tpu_custom_call" | custom-call | tf_op jit(solution)/shard_map/pallas_call | solution.py:234
  38.3 1.9 %copy-done.2 = bf16[1024,2048]{1,0:T(8,128)(2,1)} copy-done((bf16[1024,2048]{1,0:T(8,128)(2,1)}, bf16[1024,2048]{1,0:T(8,128)(2,1)S(1)}, u32[]{:S(2)}) %copy-start.2) | copy-done | bytes 4194328
  40.2 2.2 %fusion.7.refs_1_ = bf16[128,512]{1,0:T(8,128)(2,1)S(1)} fusion(bf16[128,2048]{1,0:T(8,128)(2,1)S(1)} %fusion.12.refs_0_, bf16[2048,512]{1,0:T(8,128)(2,1)} %param.30, f32[128,512]{1,0:T(8,128)S(1)} %fusion.27), kind=kOutput, calls=%fused_computation.14 | convolution fusion | flops 268828672 | bytes 3014656 | tf_op jit(solution)/shard_map/dot_general | solution.py:435
  42.5 0.0 copy-done.9
  42.5 5.9 %fusion.1 = f32[1024,512]{1,0:T(8,128)} fusion(bf16[1024,2048]{1,0:T(8,128)(2,1)} %copy-done.2, bf16[1,2048,512]{2,1,0:T(8,128)(2,1)S(1)} %copy-done.9), kind=kOutput, calls=%fused_computation.2 | convolution fusion | flops 2147483648 | bytes 8388608 | tf_op jit(solution)/shard_map/dot_general | solution.py:440
  48.4 0.0 copy-done
  48.4 10.1 %convolution_convert_fusion.refs_0_ = bf16[1024,2048]{1,0:T(8,128)(2,1)} fusion(bf16[1,512,2048]{2,1,0:T(8,128)(2,1)S(1)} %copy-done, f32[1024,512]{1,0:T(8,128)} %fusion.1, bf16[1024,2048]{1,0:T(8,128)(2,1)} %copy-done.2, bf16[1,2048,512]{2,1,0:T(8,128)(2,1)} %param.26, f32[1024]{0:T(1024)S(1)} %bitcast.30), kind=kOutput, calls=%fused_computation | convolution fusion | flops 4300734464 | bytes 14684160 | tf_op jit(solution)/shard_map/dot_general | solution.py:442
  58.5 0.0 collective-permute-done
  58.6 0.3 multiply_reduce_fusion
  58.9 0.3 copy-done.8
  59.2 2.2 %copy-done.1 = bf16[1024,2048]{1,0:T(8,128)(2,1)S(1)} copy-done((bf16[1024,2048]{1,0:T(8,128)(2,1)S(1)}, bf16[1024,2048]{1,0:T(8,128)(2,1)}, u32[]{:S(2)}) %copy-start.1) | copy-done | bytes 4194328
  61.4 33.1 %shard_map.168 = (f32[128,512]{1,0:T(8,128)S(1)}, bf16[128,2048]{1,0:T(8,128)(2,1)S(1)}, bf16[128,1024]{1,0:T(8,128)(2,1)S(1)}, f32[4,1,128]{2,1,0:T(1,128)S(1)}) custom-call(bf16[1024,2048]{1,0:T(8,128)(2,1)S(1)} %copy-done.1, bf16[128,512]{1,0:T(8,128)(2,1)S(1)} %fusion.7.refs_1_, bf16[128,256]{1,0:T(8,128)(2,1)S(1)} %multiply_convert_fusion.1.refs_2_, ...), custom_call_target="tpu_custom_call" | custom-call | tf_op jit(solution)/shard_map/pallas_call | solution.py:373
  94.6 2.2 %fusion.9 = bf16[128,512]{1,0:T(8,128)(2,1)} fusion(bf16[128,1024]{1,0:T(8,128)(2,1)S(1)} %get-tuple-element.10, bf16[1024,512]{1,0:T(8,128)(2,1)} %param.23, f32[128]{0:T(128)S(1)} %add_rsqrt_fusion), kind=kOutput, calls=%fused_computation.16 | convolution fusion | flops 134348800 | bytes 1442304 | tf_op jit(solution)/shard_map/dot_general | solution.py:448
  96.8 2.7 %fusion.8 = bf16[128,512]{1,0:T(8,128)(2,1)} fusion(f32[128,512]{1,0:T(8,128)S(1)} %get-tuple-element.12, bf16[128,2048]{1,0:T(8,128)(2,1)S(1)} %get-tuple-element.13, bf16[2048,512]{1,0:T(8,128)(2,1)} %param.31), kind=kOutput, calls=%fused_computation.15 | convolution fusion | flops 268566528 | bytes 3014656 | tf_op jit(solution)/shard_map/dot_general | solution.py:450
  (26 shorter events, 0.2 us)
Async XLA Ops:
  0.6 47.7 %copy-start = (bf16[1,512,2048]{2,1,0:T(8,128)(2,1)S(1)}, bf16[1,512,2048]{2,1,0:T(8,128)(2,1)}, u32[]{:S(2)}) copy-start(bf16[1,512,2048]{2,1,0:T(8,128)(2,1)} %param.28) | copy-start | bytes 6291460
  0.6 5.6 %copy-start.3 = (bf16[128,2048]{1,0:T(8,128)(2,1)S(1)}, bf16[128,2048]{1,0:T(8,128)(2,1)}, u32[]{:S(2)}) copy-start(bf16[128,2048]{1,0:T(8,128)(2,1)} %param.17) | copy-start | bytes 1572868
  0.7 5.9 %copy-start.5 = (f32[128,4]{0,1:T(4,128)S(1)}, f32[128,4]{0,1:T(4,128)}, u32[]{:S(2)}) copy-start(f32[128,4]{0,1:T(4,128)} %param.25) | copy-start | bytes 6148
  0.7 5.9 %copy-start.6 = (s32[128,4]{0,1:T(4,128)S(1)}, s32[128,4]{0,1:T(4,128)}, u32[]{:S(2)}) copy-start(s32[128,4]{0,1:T(4,128)} %param.24) | copy-start | bytes 6148
  0.7 5.9 %copy-start.4 = (f32[2048]{0:T(1024)S(1)}, f32[2048]{0:T(1024)}, u32[]{:S(2)}) copy-start(f32[2048]{0:T(1024)} %param.19) | copy-start | bytes 24580
  3.9 54.7 %collective-permute-start = (bf16[15,256]{1,0:T(8,128)(2,1)S(1)}, bf16[15,256]{1,0:T(8,128)(2,1)S(1)}, u32[]{:S(2)}, u32[]{:S(2)}) collective-permute-start(bf16[15,256]{1,0:T(8,128)(2,1)S(1)} %slice.69), channel_id=1, source_target_pairs={{0,4},{4,8},{8,12},{12,16},{16,20},{20,24},{24,28},{1,5},{5,9},{9,... | collective-permute-start | bytes 23048 | tf_op jit(solution)/shard_map/ppermute | solution.py:16
  38.3 1.9 %copy-start.2 = (bf16[1024,2048]{1,0:T(8,128)(2,1)}, bf16[1024,2048]{1,0:T(8,128)(2,1)S(1)}, u32[]{:S(2)}) copy-start(bf16[1024,2048]{1,0:T(8,128)(2,1)S(1)} %get-tuple-element.8) | copy-start | bytes 12582916
  40.2 2.2 %copy-start.9 = (bf16[1,2048,512]{2,1,0:T(8,128)(2,1)S(1)}, bf16[1,2048,512]{2,1,0:T(8,128)(2,1)}, u32[]{:S(2)}) copy-start(bf16[1,2048,512]{2,1,0:T(8,128)(2,1)} %param.27) | copy-start | bytes 6291460
  48.4 10.2 %copy-start.7 = (f32[256]{0:T(256)S(1)}, f32[256]{0:T(256)}, u32[]{:S(2)}) copy-start(f32[256]{0:T(256)} %param.21) | copy-start | bytes 3076
  58.5 0.7 copy-start.8
  59.2 2.2 %copy-start.1 = (bf16[1024,2048]{1,0:T(8,128)(2,1)S(1)}, bf16[1024,2048]{1,0:T(8,128)(2,1)}, u32[]{:S(2)}) copy-start(bf16[1024,2048]{1,0:T(8,128)(2,1)} %convolution_convert_fusion.refs_0_) | copy-start | bytes 12582916

commit v3 on v2

--- a/solution.py
+++ b/solution.py
@@ -142,7 +142,7 @@
     return pl.ds(pl.multiple_of(start * size, size), size)
 
 
-def gather_kernel(n_ep, m_ref, w_ref, g_ref, wg_ref, *sems):
+def gather_kernel(n_ep, m_ref, w_ref, sg_ref, su_ref, g_ref, wg_ref, sh_ref, *sems):
     (w_s, w_r, z_s, z_r, x_s, x_r, y_s, y_r, dx_s, dx_r, dy_s, dy_r, c_s, c_r) = sems
     ep, tp, z, core, xn, yn, _ = places()
     n_z = n_ep // 2
@@ -178,6 +178,16 @@
     ]
     g_ref[own_rows, :] = m_ref[...]
     wg_ref[ep] = w_ref[...]
+    tile = sg_ref.shape[1] // 2
+
+    def shared_tile(index, carry):
+        part = aligned(index, tile)
+        gate = jnp.dot(m_ref[...], sg_ref[:, part], preferred_element_type=jnp.float32)
+        upper = jnp.dot(m_ref[...], su_ref[:, part], preferred_element_type=jnp.float32)
+        sh_ref[:, part] = (gate / (1.0 + jnp.exp(-gate)) * upper).astype(jnp.bfloat16)
+        return carry
+
+    lax.fori_loop(0, 2, shared_tile, 0)
     x_copies, y_copies, dx_copies, dy_copies = {}, {}, {}, {}
 
     def block(k):
@@ -227,7 +237,7 @@
             copy.wait_send()
 
 
-def gather_rows(moe_norm, dense, n_ep):
+def gather_rows(moe_norm, dense, shared_gate, shared_up, n_ep):
     n_z = n_ep // 2
     sems = [pltpu.SemaphoreType.DMA((n_ep,))] * 2 + [pltpu.SemaphoreType.DMA((n_z,))] * 12
     vmem = pl.BlockSpec(memory_space=pltpu.VMEM)
@@ -236,17 +246,18 @@
         out_shape=(
             jax.ShapeDtypeStruct((n_ep * moe_norm.shape[0], moe_norm.shape[1]), jnp.bfloat16),
             jax.ShapeDtypeStruct((n_ep,) + dense.shape, jnp.float32),
+            jax.ShapeDtypeStruct((moe_norm.shape[0], shared_gate.shape[1]), jnp.bfloat16),
         ),
-        in_specs=[vmem] * 2,
-        out_specs=(vmem, vmem),
+        in_specs=[vmem] * 4,
+        out_specs=(vmem,) * 3,
         scratch_shapes=sems,
-        compiler_params=pltpu.CompilerParams(collective_id=0, has_side_effects=True, vmem_limit_bytes=16 << 20),
-    )(moe_norm, dense)
-
-
-def reduce_kernel(n_ep, p_ref, sh_ref, po_ref, sq_ref, o_ref, sh_all, po_all, sq_all, *scratch):
-    (ca, s, bx, by, qx, qy, r, bz) = scratch[:8]
-    (c_s, c_r, dx_s, dx_r, dy_s, dy_r, x_s, x_r, y_s, y_r, z_s, z_r, t_s, t_r) = scratch[8:]
+        compiler_params=pltpu.CompilerParams(collective_id=0, has_side_effects=True, vmem_limit_bytes=20 << 20),
+    )(moe_norm, dense, shared_gate, shared_up)
+
+
+def reduce_kernel(n_ep, h_ref, down_ref, sh_ref, po_ref, sq_ref, o_ref, sh_all, po_all, sq_all, *scratch):
+    (p, ca, s, bx, by, qx, qy, r, bz) = scratch[:9]
+    (c_s, c_r, dx_s, dx_r, dy_s, dy_r, x_s, x_r, y_s, y_r, z_s, z_r, t_s, t_r) = scratch[9:]
     ep, tp, z, core, xn, yn, dg = places()
     n_z = n_ep // 2
     rows = o_ref.shape[0]
@@ -269,18 +280,28 @@
 
     order = list(range(2, n_z - 1)) + [1, n_z - 1, 0]
     c_copies, dx_copies, dy_copies, x_copies, y_copies, z_copies = {}, {}, {}, {}, {}, {}
-    for k in order:
-        away = ((z + k) % n_z) * 2 + 1 - core
+
+    def down(k):
+        pair = aligned((z + k) % n_z, 2 * rows)
+
+        def tile(index, carry):
+            part = aligned(index, cols)
+            p[k, :, part] = jnp.dot(
+                h_ref[pair, :], down_ref[:, part], preferred_element_type=jnp.float32
+            ).astype(jnp.bfloat16)
+            return carry
+
+        lax.fori_loop(0, down_ref.shape[1] // cols, tile, 0)
         c_copies[k] = send(
-            p_ref.at[aligned(away, rows), :], ca.at[k], c_s.at[k], c_r.at[k], (other_core, tp)
-        )
+            p.at[k, aligned(1 - core, rows), :], ca.at[k], c_s.at[k], c_r.at[k], (other_core, tp)
+        )
+
     low, high = pl.ds(0, half), pl.ds(half, half)
 
     def first(k):
         c_copies[k].wait_recv()
-        mine = ((z + k) % n_z) * 2 + core
         s[k] = (
-            p_ref[aligned(mine, rows), :].astype(jnp.float32) + ca[k].astype(jnp.float32)
+            p[k, aligned(core, rows), :].astype(jnp.float32) + ca[k].astype(jnp.float32)
         ).astype(jnp.bfloat16)
         dx_copies[k] = send(
             s.at[k, low, aligned(dg, cols)], bx.at[k], dx_s.at[k], dx_r.at[k], (ep, xn)
@@ -321,7 +342,10 @@
             z_copies[k] = send(r.at[k], bz.at[k], z_s.at[k], z_r.at[k], (target, tp))
 
     t_copies = []
+    down(order[0])
     for index in range(n_z + 2):
+        if index + 1 < n_z:
+            down(order[index + 1])
         if index < n_z:
             first(order[index])
         if 1 <= index < n_z + 1:
@@ -352,14 +376,15 @@
             copy.wait_send()
 
 
-def reduce_rows(weighted, shared_hidden, pooled, squares, n_ep, n_tp):
+def reduce_rows(hidden, down, shared_hidden, pooled, squares, n_ep, n_tp):
     n_z = n_ep // 2
-    rows, width = weighted.shape[0] // n_ep, weighted.shape[1]
+    rows, width = hidden.shape[0] // n_ep, down.shape[1]
     cols = width // n_tp
     half = rows // 2
     bf16 = jnp.bfloat16
     vmem = pl.BlockSpec(memory_space=pltpu.VMEM)
     scratch = [
+        pltpu.VMEM((n_z, 2 * rows, width), bf16),
         pltpu.VMEM((n_z, rows, width), bf16),
         pltpu.VMEM((n_z, rows, width), bf16),
         pltpu.VMEM((n_z, half, cols), bf16),
@@ -378,13 +403,13 @@
             jax.ShapeDtypeStruct((rows, n_tp * pooled.shape[1]), bf16),
             jax.ShapeDtypeStruct((n_tp,) + squares.shape, jnp.float32),
         ),
-        in_specs=[vmem] * 4,
+        in_specs=[vmem] * 5,
         out_specs=(vmem,) * 4,
         scratch_shapes=scratch + sems,
         compiler_params=pltpu.CompilerParams(
-            collective_id=1, has_side_effects=True, vmem_limit_bytes=16 << 20
+            collective_id=1, has_side_effects=True, vmem_limit_bytes=24 << 20
         ),
-    )(weighted, shared_hidden, pooled, squares)
+    )(hidden, down, shared_hidden, pooled, squares)
 
 
 def dense_on_device(
@@ -421,7 +446,9 @@
     mix_norm = row_norm(mix_input, mix_gain)
     pool_input = jnp.dot(mix_norm, pool_in, preferred_element_type=f32).astype(jnp.bfloat16)
     before = shifted(pool_input[tok_rows - reach_rows :], "ep", 1)
-    all_rows, all_weights = gather_rows(moe_norm, dense, n_ep)
+    all_rows, all_weights, shared_hidden = gather_rows(
+        moe_norm, dense, shared_gate, shared_up, n_ep
+    )
 
     extended = jnp.concatenate([before, pool_input], axis=0).astype(f32)
     position = (me * tok_rows + jnp.arange(tok_rows, dtype=jnp.int32) + 1).astype(f32)
@@ -430,18 +457,12 @@
     scaled = window_means(extended, position, group, tok_rows) * pool_scale
     squares = jnp.sum(scaled * scaled, axis=1)[None, :]
     pooled = (scaled * pool_gain).astype(jnp.bfloat16)
-    shared_hidden = (
-        jax.nn.silu(jnp.dot(moe_norm, shared_gate, preferred_element_type=f32))
-        * jnp.dot(moe_norm, shared_up, preferred_element_type=f32)
-    ).astype(jnp.bfloat16)
-
     factor = lax.dynamic_index_in_dim(all_weights, me, axis=1, keepdims=False).reshape(-1, 1)
     gate = jnp.dot(all_rows, expert_gate[0], preferred_element_type=f32)
     upper = jnp.dot(all_rows, expert_up[0], preferred_element_type=f32)
     hidden = (jax.nn.silu(gate) * upper * factor).astype(jnp.bfloat16)
-    weighted = jnp.dot(hidden, expert_down[0], preferred_element_type=f32).astype(jnp.bfloat16)
     routed, shared_all, pooled_all, squares_all = reduce_rows(
-        weighted, shared_hidden, pooled, squares, n_ep, n_tp
+        hidden, expert_down[0], shared_hidden, pooled, squares, n_ep, n_tp
     )
     mean = jnp.sum(squares_all, axis=0).reshape(-1, 1) / pool_width
     mix_out = (

time: 99.8 us -> 92.3 us (0.925)
  matrix products: 26.9 us -> 16.4 us
  local copies, waits for them, and re-layouts: 4.46 us -> 6.34 us
  Pallas kernels: 62.6 us -> 63.7 us
    dot_general x3 -> x1, matrix products: 14.3 us -> 6.11 us  [dense_on_device(): gate = jnp.dot(all_rows, expert_gate[0], preferred_element_type=f32)]
    dot_general x1, matrix products: 5.91 us -> 3.66 us  [dense_on_device(): upper = jnp.dot(all_rows, expert_up[0], preferred_element_type=f32)]
    unnamed x20 -> x22, local copies, waits for them, and re-layouts: 4.44 us -> 6.32 us
    pallas_call x1, Pallas kernels: 33.1 us -> 34.4 us  [reduce_rows(): pl.pallas_call(lambda *refs: reduce_kernel(n_ep, *refs), out_shape=(jax.S...]
  transfers between devices with their start and end apart: 1 -> 1, of which waited for: 0 -> 0; matrix products, arithmetic and copies ran while one was open for 21% -> 11% of each run, Pallas kernels for 30% -> 32%
where the time goes in v3:
time: 92.3 us; the launch traced here: 92 us
  Pallas kernels  63.7 us (69%)
  matrix products  16.4 us (18%)
  local copies, waits for them, and re-layouts  6.34 us (7%)
  starting transfers between devices  2.4 us (3%)
  other arithmetic  2.24 us (2%)
    pallas_call x1, Pallas kernels, reduce_rows(): pl.pallas_call(lambda *refs: reduce_kernel(n_ep, *refs), out_shape=(jax.S...  34.4 us
    pallas_call x1, Pallas kernels, gather_rows(): pl.pallas_call(lambda *refs: gather_kernel(n_ep, *refs), out_shape=(jax.S...  29.3 us
    unnamed x22, local copies, waits for them, and re-layouts  6.32 us
    dot_general x1, matrix products, dense_on_device(): gate = jnp.dot(all_rows, expert_gate[0], preferred_element_type=f32)  6.11 us
    dot_general x1, matrix products, dense_on_device(): upper = jnp.dot(all_rows, expert_up[0], preferred_element_type=f32)  3.66 us
    dot_general x1, matrix products, dense_on_device(): shared_part = jnp.dot(shared_all, shared_down, preferred_element_type=f32)  2.7 us
    ppermute x1, starting transfers between devices, shifted(): return lax.ppermute(block, axis, route)  2.4 us
    dot_general x1, matrix products, dense_on_device(): jnp.dot(pooled_all, pool_out, preferred_element_type=f32)  2.2 us
  transfers between devices with their start and end apart: 1, of which 0 were waited for; matrix products, arithmetic and copies ran while one was open for 11% of the time, Pallas kernels for 32%

profile of v3, /device:TPU:0, one launch (start us, length us, event | category | flops | bytes accessed | tf_op | source)
XLA Modules:
  0.0 92.0 jit_solution(5691516124526159760)
XLA Ops:
  0.6 0.0 copy-start
  0.6 0.0 copy-start.5
  0.7 0.0 copy-start.7
  0.7 1.4 %fusion.11 = f32[128]{0:T(128)S(1)} fusion(bf16[128,2048]{1,0:T(8,128)(2,1)} %param.16), kind=kLoop, calls=%fused_computation.17 | loop fusion | flops 786304 | bytes 524800 | tf_op jit(solution)/shard_map/reduce_sum | solution.py:21
  2.1 1.8 %convolution_convert_fusion = bf16[128,256]{1,0:T(8,128)(2,1)S(1)} fusion(bf16[2048,256]{1,0:T(8,128)(2,1)} %param.20, bf16[128,2048]{1,0:T(8,128)(2,1)} %param.16, f32[2048]{0:T(1024)} %param.18, f32[128]{0:T(128)S(1)} %add_rsqrt_fusion.1), kind=kOutput, calls=%fused_computation.13 | convolution fusion | flops 135299072 | bytes 1647104 | tf_op jit(solution)/shard_map/dot_general | solution.py:447
  3.9 2.4 %collective-permute-start = (bf16[15,256]{1,0:T(8,128)(2,1)S(1)}, bf16[15,256]{1,0:T(8,128)(2,1)S(1)}, u32[]{:S(2)}, u32[]{:S(2)}) collective-permute-start(bf16[15,256]{1,0:T(8,128)(2,1)S(1)} %slice.69), channel_id=1, source_target_pairs={{0,4},{4,8},{8,12},{12,16},{16,20},{20,24},{24,28},{1,5},{5,9},{9,... | collective-permute-start | bytes 23048 | tf_op jit(solution)/shard_map/ppermute | solution.py:16
  6.3 0.2 fusion.8
  6.6 0.2 fusion.10.refs_0_
  6.8 0.0 copy-start.2
  6.8 1.6 %copy-done.2 = bf16[2048,512]{1,0:T(8,128)(2,1)S(1)} copy-done((bf16[2048,512]{1,0:T(8,128)(2,1)S(1)}, bf16[2048,512]{1,0:T(8,128)(2,1)}, u32[]{:S(2)}) %copy-start.2) | copy-done | bytes 2097176
  8.4 1.6 %copy-done.3 = bf16[2048,512]{1,0:T(8,128)(2,1)S(1)} copy-done((bf16[2048,512]{1,0:T(8,128)(2,1)S(1)}, bf16[2048,512]{1,0:T(8,128)(2,1)}, u32[]{:S(2)}) %copy-start.3) | copy-done | bytes 2097176
  10.0 29.3 %shard_map.167 = (bf16[1024,2048]{1,0:T(8,128)(2,1)S(1)}, f32[8,8,128]{2,1,0:T(8,128)S(1)}, bf16[128,512]{1,0:T(8,128)(2,1)S(1)}) custom-call(bf16[128,2048]{1,0:T(8,128)(2,1)S(1)} %fusion.10.refs_0_, f32[8,128]{1,0:T(8,128)S(1)} %select_reduce_fusion.refs_1_, bf16[2048,512]{1,0:T(8,128)(2,1)S(1)} %copy-done.2, bf16[2048,512]{1,0:T(8,128)(2,1)S(1)} %copy-done.3), custom_call_target="tpu_custom_call" | custom-call | tf_op jit(solution)/shard_map/pallas_call | solution.py:244
  39.3 1.9 %copy-done.4 = bf16[1024,2048]{1,0:T(8,128)(2,1)} copy-done((bf16[1024,2048]{1,0:T(8,128)(2,1)}, bf16[1024,2048]{1,0:T(8,128)(2,1)S(1)}, u32[]{:S(2)}) %copy-start.4) | copy-done | bytes 4194328
  41.2 3.7 %fusion = f32[1024,512]{1,0:T(8,128)} fusion(bf16[1024,2048]{1,0:T(8,128)(2,1)S(1)} %get-tuple-element.9, bf16[1,2048,512]{2,1,0:T(8,128)(2,1)S(1)} %copy-done), kind=kOutput, calls=%fused_computation | convolution fusion | flops 2147483648 | bytes 8388608 | tf_op jit(solution)/shard_map/dot_general | solution.py:462
  44.9 6.1 %multiply_convert_fusion.refs_0_ = bf16[1024,512]{1,0:T(8,128)(2,1)S(1)} fusion(f32[1024,512]{1,0:T(8,128)} %fusion, bf16[1024,2048]{1,0:T(8,128)(2,1)} %copy-done.4, bf16[1,2048,512]{2,1,0:T(8,128)(2,1)} %param.26, f32[1024]{0:T(1024)S(1)} %bitcast.23), kind=kOutput, calls=%fused_computation.4 | convolution fusion | flops 2151153664 | bytes 9441280 | tf_op jit(solution)/shard_map/dot_general | solution.py:461
  51.0 0.0 copy-start.10
  51.0 0.0 copy-start.1
  51.1 0.0 collective-permute-done
  51.1 0.3 multiply_reduce_fusion
  51.4 0.3 copy-done.10
  51.7 0.9 copy-done.1
  52.6 34.4 %shard_map.168 = (f32[128,512]{1,0:T(8,128)S(1)}, bf16[128,2048]{1,0:T(8,128)(2,1)S(1)}, bf16[128,1024]{1,0:T(8,128)(2,1)S(1)}, f32[4,1,128]{2,1,0:T(1,128)S(1)}) custom-call(bf16[1024,512]{1,0:T(8,128)(2,1)S(1)} %multiply_convert_fusion.refs_0_, bf16[512,2048]{1,0:T(8,128)(2,1)S(1)} %bitcast.21, bf16[128,512]{1,0:T(8,128)(2,1)S(1)} %get-tuple-element.11.refs_2_, ...), custom_call_target="tpu_custom_call" | custom-call | tf_op jit(solution)/shard_map/pallas_call | solution.py:398
  87.1 2.2 %fusion.7 = bf16[128,512]{1,0:T(8,128)(2,1)} fusion(bf16[128,1024]{1,0:T(8,128)(2,1)S(1)} %get-tuple-element.12, bf16[1024,512]{1,0:T(8,128)(2,1)} %param.23, f32[128]{0:T(128)S(1)} %add_rsqrt_fusion), kind=kOutput, calls=%fused_computation.12 | convolution fusion | flops 134348800 | bytes 1442304 | tf_op jit(solution)/shard_map/dot_general | solution.py:469
  89.3 2.7 %fusion.6 = bf16[128,512]{1,0:T(8,128)(2,1)} fusion(f32[128,512]{1,0:T(8,128)S(1)} %get-tuple-element.14, bf16[128,2048]{1,0:T(8,128)(2,1)S(1)} %get-tuple-element.15, bf16[2048,512]{1,0:T(8,128)(2,1)} %param.31), kind=kOutput, calls=%fused_computation.11 | convolution fusion | flops 268566528 | bytes 3014656 | tf_op jit(solution)/shard_map/dot_general | solution.py:471
  (26 shorter events, 0.2 us)
Async XLA Ops:
  0.6 40.6 %copy-start = (bf16[1,2048,512]{2,1,0:T(8,128)(2,1)S(1)}, bf16[1,2048,512]{2,1,0:T(8,128)(2,1)}, u32[]{:S(2)}) copy-start(bf16[1,2048,512]{2,1,0:T(8,128)(2,1)} %param.27) | copy-start | bytes 6291460
  0.6 5.6 %copy-start.5 = (bf16[128,2048]{1,0:T(8,128)(2,1)S(1)}, bf16[128,2048]{1,0:T(8,128)(2,1)}, u32[]{:S(2)}) copy-start(bf16[128,2048]{1,0:T(8,128)(2,1)} %param.17) | copy-start | bytes 1572868
  0.7 5.8 %copy-start.7 = (f32[128,4]{0,1:T(4,128)S(1)}, f32[128,4]{0,1:T(4,128)}, u32[]{:S(2)}) copy-start(f32[128,4]{0,1:T(4,128)} %param.25) | copy-start | bytes 6148
  0.7 5.9 %copy-start.6 = (f32[2048]{0:T(1024)S(1)}, f32[2048]{0:T(1024)}, u32[]{:S(2)}) copy-start(f32[2048]{0:T(1024)} %param.19) | copy-start | bytes 24580
  0.7 6.1 %copy-start.8 = (s32[128,4]{0,1:T(4,128)S(1)}, s32[128,4]{0,1:T(4,128)}, u32[]{:S(2)}) copy-start(s32[128,4]{0,1:T(4,128)} %param.24) | copy-start | bytes 6148
  3.9 47.2 %collective-permute-start = (bf16[15,256]{1,0:T(8,128)(2,1)S(1)}, bf16[15,256]{1,0:T(8,128)(2,1)S(1)}, u32[]{:S(2)}, u32[]{:S(2)}) collective-permute-start(bf16[15,256]{1,0:T(8,128)(2,1)S(1)} %slice.69), channel_id=1, source_target_pairs={{0,4},{4,8},{8,12},{12,16},{16,20},{20,24},{24,28},{1,5},{5,9},{9,... | collective-permute-start | bytes 23048 | tf_op jit(solution)/shard_map/ppermute | solution.py:16
  6.8 1.6 %copy-start.2 = (bf16[2048,512]{1,0:T(8,128)(2,1)S(1)}, bf16[2048,512]{1,0:T(8,128)(2,1)}, u32[]{:S(2)}) copy-start(bf16[2048,512]{1,0:T(8,128)(2,1)} %refs_2_.1) | copy-start | bytes 6291460
  8.4 1.6 %copy-start.3 = (bf16[2048,512]{1,0:T(8,128)(2,1)S(1)}, bf16[2048,512]{1,0:T(8,128)(2,1)}, u32[]{:S(2)}) copy-start(bf16[2048,512]{1,0:T(8,128)(2,1)} %refs_3_.1) | copy-start | bytes 6291460
  39.3 1.9 %copy-start.4 = (bf16[1024,2048]{1,0:T(8,128)(2,1)}, bf16[1024,2048]{1,0:T(8,128)(2,1)S(1)}, u32[]{:S(2)}) copy-start(bf16[1024,2048]{1,0:T(8,128)(2,1)S(1)} %get-tuple-element.9) | copy-start | bytes 12582916
  44.9 6.2 %copy-start.9 = (f32[256]{0:T(256)S(1)}, f32[256]{0:T(256)}, u32[]{:S(2)}) copy-start(f32[256]{0:T(256)} %param.21) | copy-start | bytes 3076
  51.0 0.7 copy-start.10
  51.0 1.6 %copy-start.1 = (bf16[1,512,2048]{2,1,0:T(8,128)(2,1)S(1)}, bf16[1,512,2048]{2,1,0:T(8,128)(2,1)}, u32[]{:S(2)}) copy-start(bf16[1,512,2048]{2,1,0:T(8,128)(2,1)} %param.28) | copy-start | bytes 6291460

commit v4 on v3

--- a/solution.py
+++ b/solution.py
@@ -142,8 +142,15 @@
     return pl.ds(pl.multiple_of(start * size, size), size)
 
 
-def gather_kernel(n_ep, m_ref, w_ref, sg_ref, su_ref, g_ref, wg_ref, sh_ref, *sems):
-    (w_s, w_r, z_s, z_r, x_s, x_r, y_s, y_r, dx_s, dx_r, dy_s, dy_r, c_s, c_r) = sems
+def gather_kernel(n_ep, m_ref, w_ref, sg_hbm, su_hbm, g_ref, wg_ref, sh_ref, *scratch):
+    (w_s, w_r, z_s, z_r, x_s, x_r, y_s, y_r, dx_s, dx_r, dy_s, dy_r, c_s, c_r) = scratch[:14]
+    sg_ref, su_ref, load = scratch[14:]
+    loads = [
+        pltpu.make_async_copy(sg_hbm, sg_ref, load.at[0]),
+        pltpu.make_async_copy(su_hbm, su_ref, load.at[1]),
+    ]
+    for copy in loads:
+        copy.start()
     ep, tp, z, core, xn, yn, _ = places()
     n_z = n_ep // 2
     rows = m_ref.shape[0]
@@ -187,6 +194,8 @@
         sh_ref[:, part] = (gate / (1.0 + jnp.exp(-gate)) * upper).astype(jnp.bfloat16)
         return carry
 
+    for copy in loads:
+        copy.wait()
     lax.fori_loop(0, 2, shared_tile, 0)
     x_copies, y_copies, dx_copies, dy_copies = {}, {}, {}, {}
 
@@ -240,6 +249,11 @@
 def gather_rows(moe_norm, dense, shared_gate, shared_up, n_ep):
     n_z = n_ep // 2
     sems = [pltpu.SemaphoreType.DMA((n_ep,))] * 2 + [pltpu.SemaphoreType.DMA((n_z,))] * 12
+    sems = sems + [
+        pltpu.VMEM(shared_gate.shape, jnp.bfloat16),
+        pltpu.VMEM(shared_up.shape, jnp.bfloat16),
+        pltpu.SemaphoreType.DMA((2,)),
+    ]
     vmem = pl.BlockSpec(memory_space=pltpu.VMEM)
     return pl.pallas_call(
         lambda *refs: gather_kernel(n_ep, *refs),
@@ -248,7 +262,7 @@
             jax.ShapeDtypeStruct((n_ep,) + dense.shape, jnp.float32),
             jax.ShapeDtypeStruct((moe_norm.shape[0], shared_gate.shape[1]), jnp.bfloat16),
         ),
-        in_specs=[vmem] * 4,
+        in_specs=[vmem] * 2 + [pl.BlockSpec(memory_space=pltpu.HBM)] * 2,
         out_specs=(vmem,) * 3,
         scratch_shapes=sems,
         compiler_params=pltpu.CompilerParams(collective_id=0, has_side_effects=True, vmem_limit_bytes=20 << 20),

time: 92.3 us -> 92.7 us (level)
  no operation moved by 1% of the time
where the time goes in v4:
time: 92.7 us; the launch traced here: 92.3 us
  Pallas kernels  64.1 us (69%)
  matrix products  16.4 us (18%)
  local copies, waits for them, and re-layouts  6.34 us (7%)
  starting transfers between devices  2.4 us (3%)
  other arithmetic  2.24 us (2%)
    pallas_call x1, Pallas kernels, reduce_rows(): pl.pallas_call(lambda *refs: reduce_kernel(n_ep, *refs), out_shape=(jax.S...  34.4 us
    pallas_call x1, Pallas kernels, gather_rows(): pl.pallas_call(lambda *refs: gather_kernel(n_ep, *refs), out_shape=(jax.S...  29.7 us
    unnamed x22, local copies, waits for them, and re-layouts  6.32 us
    dot_general x1, matrix products, dense_on_device(): gate = jnp.dot(all_rows, expert_gate[0], preferred_element_type=f32)  6.1 us
    dot_general x1, matrix products, dense_on_device(): upper = jnp.dot(all_rows, expert_up[0], preferred_element_type=f32)  3.65 us
    dot_general x1, matrix products, dense_on_device(): shared_part = jnp.dot(shared_all, shared_down, preferred_element_type=f32)  2.7 us
    ppermute x1, starting transfers between devices, shifted(): return lax.ppermute(block, axis, route)  2.4 us
    dot_general x1, matrix products, dense_on_device(): jnp.dot(pooled_all, pool_out, preferred_element_type=f32)  2.2 us
  transfers between devices with their start and end apart: 1, of which 0 were waited for; matrix products, arithmetic and copies ran while one was open for 11% of the time, Pallas kernels for 32%

profile of v4, /device:TPU:0, one launch (start us, length us, event | category | flops | bytes accessed | tf_op | source)
XLA Modules:
  0.0 92.3 jit_solution(16647710556781144896)
XLA Ops:
  0.6 0.0 copy-start
  0.6 0.0 copy-start.5
  0.7 1.4 %fusion.11 = f32[128]{0:T(128)S(1)} fusion(bf16[128,2048]{1,0:T(8,128)(2,1)} %param.16), kind=kLoop, calls=%fused_computation.17 | loop fusion | flops 786304 | bytes 524800 | tf_op jit(solution)/shard_map/reduce_sum | solution.py:21
  2.1 1.8 %convolution_convert_fusion = bf16[128,256]{1,0:T(8,128)(2,1)S(1)} fusion(bf16[2048,256]{1,0:T(8,128)(2,1)} %param.20, bf16[128,2048]{1,0:T(8,128)(2,1)} %param.16, f32[2048]{0:T(1024)} %param.18, f32[128]{0:T(128)S(1)} %add_rsqrt_fusion.1), kind=kOutput, calls=%fused_computation.13 | convolution fusion | flops 135299072 | bytes 1647104 | tf_op jit(solution)/shard_map/dot_general | solution.py:461
  3.9 2.4 %collective-permute-start = (bf16[15,256]{1,0:T(8,128)(2,1)S(1)}, bf16[15,256]{1,0:T(8,128)(2,1)S(1)}, u32[]{:S(2)}, u32[]{:S(2)}) collective-permute-start(bf16[15,256]{1,0:T(8,128)(2,1)S(1)} %slice.69), channel_id=1, source_target_pairs={{0,4},{4,8},{8,12},{12,16},{16,20},{20,24},{24,28},{1,5},{5,9},{9,... | collective-permute-start | bytes 23048 | tf_op jit(solution)/shard_map/ppermute | solution.py:16
  6.3 0.2 fusion.8
  6.6 0.0 copy-done.6
  6.6 0.2 fusion.10.refs_0_
  6.8 0.0 copy-start.2
  6.8 1.6 %copy-done.2 = bf16[2048,512]{1,0:T(8,128)(2,1)S(1)} copy-done((bf16[2048,512]{1,0:T(8,128)(2,1)S(1)}, bf16[2048,512]{1,0:T(8,128)(2,1)}, u32[]{:S(2)}) %copy-start.2) | copy-done | bytes 2097176
  8.4 1.6 %copy-done.3 = bf16[2048,512]{1,0:T(8,128)(2,1)S(1)} copy-done((bf16[2048,512]{1,0:T(8,128)(2,1)S(1)}, bf16[2048,512]{1,0:T(8,128)(2,1)}, u32[]{:S(2)}) %copy-start.3) | copy-done | bytes 2097176
  10.0 29.7 %shard_map.167 = (bf16[1024,2048]{1,0:T(8,128)(2,1)S(1)}, f32[8,8,128]{2,1,0:T(8,128)S(1)}, bf16[128,512]{1,0:T(8,128)(2,1)S(1)}) custom-call(bf16[128,2048]{1,0:T(8,128)(2,1)S(1)} %fusion.10.refs_0_, f32[8,128]{1,0:T(8,128)S(1)} %select_reduce_fusion.refs_1_, bf16[2048,512]{1,0:T(8,128)(2,1)S(1)} %copy-done.2, bf16[2048,512]{1,0:T(8,128)(2,1)S(1)} %copy-done.3), custom_call_target="tpu_custom_call" | custom-call | tf_op jit(solution)/shard_map/pallas_call | solution.py:258
  39.7 1.9 %copy-done.4 = bf16[1024,2048]{1,0:T(8,128)(2,1)} copy-done((bf16[1024,2048]{1,0:T(8,128)(2,1)}, bf16[1024,2048]{1,0:T(8,128)(2,1)S(1)}, u32[]{:S(2)}) %copy-start.4) | copy-done | bytes 4194328
  41.7 3.6 %fusion = f32[1024,512]{1,0:T(8,128)} fusion(bf16[1024,2048]{1,0:T(8,128)(2,1)S(1)} %get-tuple-element.9, bf16[1,2048,512]{2,1,0:T(8,128)(2,1)S(1)} %copy-done), kind=kOutput, calls=%fused_computation | convolution fusion | flops 2147483648 | bytes 8388608 | tf_op jit(solution)/shard_map/dot_general | solution.py:476
  45.3 6.1 %multiply_convert_fusion.refs_0_ = bf16[1024,512]{1,0:T(8,128)(2,1)S(1)} fusion(f32[1024,512]{1,0:T(8,128)} %fusion, bf16[1024,2048]{1,0:T(8,128)(2,1)} %copy-done.4, bf16[1,2048,512]{2,1,0:T(8,128)(2,1)} %param.26, f32[1024]{0:T(1024)S(1)} %bitcast.23), kind=kOutput, calls=%fused_computation.4 | convolution fusion | flops 2151153664 | bytes 9441280 | tf_op jit(solution)/shard_map/dot_general | solution.py:475
  51.4 0.0 copy-start.10
  51.4 0.0 copy-start.1
  51.5 0.0 collective-permute-done
  51.5 0.3 multiply_reduce_fusion
  51.8 0.3 copy-done.10
  52.1 0.9 copy-done.1
  53.0 34.4 %shard_map.168 = (f32[128,512]{1,0:T(8,128)S(1)}, bf16[128,2048]{1,0:T(8,128)(2,1)S(1)}, bf16[128,1024]{1,0:T(8,128)(2,1)S(1)}, f32[4,1,128]{2,1,0:T(1,128)S(1)}) custom-call(bf16[1024,512]{1,0:T(8,128)(2,1)S(1)} %multiply_convert_fusion.refs_0_, bf16[512,2048]{1,0:T(8,128)(2,1)S(1)} %bitcast.21, bf16[128,512]{1,0:T(8,128)(2,1)S(1)} %get-tuple-element.11.refs_2_, ...), custom_call_target="tpu_custom_call" | custom-call | tf_op jit(solution)/shard_map/pallas_call | solution.py:412
  87.4 2.2 %fusion.7 = bf16[128,512]{1,0:T(8,128)(2,1)} fusion(bf16[128,1024]{1,0:T(8,128)(2,1)S(1)} %get-tuple-element.12, bf16[1024,512]{1,0:T(8,128)(2,1)} %param.23, f32[128]{0:T(128)S(1)} %add_rsqrt_fusion), kind=kOutput, calls=%fused_computation.12 | convolution fusion | flops 134348800 | bytes 1442304 | tf_op jit(solution)/shard_map/dot_general | solution.py:483
  89.6 2.7 %fusion.6 = bf16[128,512]{1,0:T(8,128)(2,1)} fusion(f32[128,512]{1,0:T(8,128)S(1)} %get-tuple-element.14, bf16[128,2048]{1,0:T(8,128)(2,1)S(1)} %get-tuple-element.15, bf16[2048,512]{1,0:T(8,128)(2,1)} %param.31), kind=kOutput, calls=%fused_computation.11 | convolution fusion | flops 268566528 | bytes 3014656 | tf_op jit(solution)/shard_map/dot_general | solution.py:485
  (26 shorter events, 0.2 us)
Async XLA Ops:
  0.6 41.0 %copy-start = (bf16[1,2048,512]{2,1,0:T(8,128)(2,1)S(1)}, bf16[1,2048,512]{2,1,0:T(8,128)(2,1)}, u32[]{:S(2)}) copy-start(bf16[1,2048,512]{2,1,0:T(8,128)(2,1)} %param.27) | copy-start | bytes 6291460
  0.6 5.6 %copy-start.5 = (bf16[128,2048]{1,0:T(8,128)(2,1)S(1)}, bf16[128,2048]{1,0:T(8,128)(2,1)}, u32[]{:S(2)}) copy-start(bf16[128,2048]{1,0:T(8,128)(2,1)} %param.17) | copy-start | bytes 1572868
  0.7 5.8 %copy-start.7 = (f32[128,4]{0,1:T(4,128)S(1)}, f32[128,4]{0,1:T(4,128)}, u32[]{:S(2)}) copy-start(f32[128,4]{0,1:T(4,128)} %param.25) | copy-start | bytes 6148
  0.7 5.9 %copy-start.6 = (f32[2048]{0:T(1024)S(1)}, f32[2048]{0:T(1024)}, u32[]{:S(2)}) copy-start(f32[2048]{0:T(1024)} %param.19) | copy-start | bytes 24580
  0.7 6.1 %copy-start.8 = (s32[128,4]{0,1:T(4,128)S(1)}, s32[128,4]{0,1:T(4,128)}, u32[]{:S(2)}) copy-start(s32[128,4]{0,1:T(4,128)} %param.24) | copy-start | bytes 6148
  3.9 47.6 %collective-permute-start = (bf16[15,256]{1,0:T(8,128)(2,1)S(1)}, bf16[15,256]{1,0:T(8,128)(2,1)S(1)}, u32[]{:S(2)}, u32[]{:S(2)}) collective-permute-start(bf16[15,256]{1,0:T(8,128)(2,1)S(1)} %slice.69), channel_id=1, source_target_pairs={{0,4},{4,8},{8,12},{12,16},{16,20},{20,24},{24,28},{1,5},{5,9},{9,... | collective-permute-start | bytes 23048 | tf_op jit(solution)/shard_map/ppermute | solution.py:16
  6.8 1.6 %copy-start.2 = (bf16[2048,512]{1,0:T(8,128)(2,1)S(1)}, bf16[2048,512]{1,0:T(8,128)(2,1)}, u32[]{:S(2)}) copy-start(bf16[2048,512]{1,0:T(8,128)(2,1)} %refs_2_.1) | copy-start | bytes 6291460
  8.4 1.6 %copy-start.3 = (bf16[2048,512]{1,0:T(8,128)(2,1)S(1)}, bf16[2048,512]{1,0:T(8,128)(2,1)}, u32[]{:S(2)}) copy-start(bf16[2048,512]{1,0:T(8,128)(2,1)} %refs_3_.1) | copy-start | bytes 6291460
  39.7 1.9 %copy-start.4 = (bf16[1024,2048]{1,0:T(8,128)(2,1)}, bf16[1024,2048]{1,0:T(8,128)(2,1)S(1)}, u32[]{:S(2)}) copy-start(bf16[1024,2048]{1,0:T(8,128)(2,1)S(1)} %get-tuple-element.9) | copy-start | bytes 12582916
  45.3 6.2 %copy-start.9 = (f32[256]{0:T(256)S(1)}, f32[256]{0:T(256)}, u32[]{:S(2)}) copy-start(f32[256]{0:T(256)} %param.21) | copy-start | bytes 3076
  51.4 0.7 copy-start.10
  51.4 1.6 %copy-start.1 = (bf16[1,512,2048]{2,1,0:T(8,128)(2,1)S(1)}, bf16[1,512,2048]{2,1,0:T(8,128)(2,1)}, u32[]{:S(2)}) copy-start(bf16[1,512,2048]{2,1,0:T(8,128)(2,1)} %param.28) | copy-start | bytes 6291460
